TPU v7x, 256 devices: a whole 4x4x8 slice. The times are simulated.
256 devices in a mesh: tp: 16 (over y, x), dp: 16 (over z, core).
Axes of the slice: x: 4, y: 4, z: 8, core: 2. Of those that a mesh axis runs over, the one named last changes fastest.
Arguments:
- tokens: bfloat16 [256, 4096], P(None, 'dp'), may hold values from -15 to 15, as said below
- norm_gain: float32 [2, 4096], P(None, 'dp'), may hold values from 0.1 to 1.9
- w_query: bfloat16 [2, 4096, 2048], P(None, 'dp', 'tp'), may hold values from -0.09375 to 0.09375
- w_forget: bfloat16 [2, 4096, 2048], P(None, 'dp', 'tp'), may hold values from -0.09375 to 0.09375
- w_value: bfloat16 [2, 4096, 2048], P(None, 'dp', 'tp'), may hold values from -0.09375 to 0.09375
- w_gate: bfloat16 [2, 4096, 2048], P(None, 'dp', 'tp'), may hold values from -0.09375 to 0.09375
- floor_rate: float32 [2, 2048], P(None, 'tp'), may hold values from 0 to 0.9
- head_gain: float32 [2, 128], replicated, may hold values from 0.1 to 1.9
- w_output: bfloat16 [2, 2048, 4096], P(None, 'tp', 'dp'), may hold values from -0.3 to 0.3
- state: float32 [2, 256, 16, 128, 128], P(None, 'dp', 'tp'), may hold values from -4 to 4
Outputs:
- mixed: bfloat16 [256, 4096], P(None, 'dp')
- new_state: float32 [2, 256, 16, 128, 128], P(None, 'dp', 'tp')
Inputs may be any that keep to these rules, and one draw needn't show every extreme that they name: `tokens`: activations whose feature blocks have different scales.
All inputs are finite; a program needn't handle non-finite values.
Results may differ from a plain program's by a relative error of at most 0.035.
Values may be sent and summed in bfloat16 or wider, within the bound.
A program may use at most 64 MiB of HBM per device.

v0:
```python
import jax
import jax.numpy as jnp
from jax import lax
from jax.sharding import PartitionSpec as P

D = 4096
DK = 128


EPS = 1e-06


def cut_along(x, dim, length):
    lengths = x.shape
    parts = x.reshape(*lengths[:dim], length, lengths[dim] // length, *lengths[dim + 1 :])
    return jnp.moveaxis(parts, dim, 0)


def summed_on_arrival(x, axis, dim):
    parts = cut_along(x, dim, lax.axis_size(axis))
    arrived = lax.all_to_all(parts, axis, split_axis=0, concat_axis=0, tiled=True)
    return arrived.sum(axis=0)


def summed_on_arrival_2(x, axis, dim):
    parts = cut_along(x, dim, lax.axis_size(axis))
    arrived = lax.all_to_all(parts, axis, split_axis=0, concat_axis=0, tiled=True)
    return arrived.astype(jnp.float32).sum(axis=0)


def from_everyone(x, axis):
    copies = jnp.broadcast_to(x, (lax.axis_size(axis), *x.shape))
    return lax.all_to_all(copies, axis, split_axis=0, concat_axis=0, tiled=True)


def laid_out(parts, dim):
    parts = jnp.moveaxis(parts, 0, dim)
    lengths = parts.shape
    return parts.reshape(*lengths[:dim], lengths[dim] * lengths[dim + 1], *lengths[dim + 2 :])


def gather_directly(x, axis, dim):
    parts = from_everyone(x, axis)
    return laid_out(parts, dim)


def mixer_layer(tokens, norm_gain, weights, floor_rate, head_gain, w_output, old_state):
    tok = tokens.astype(jnp.float32)
    squares = summed_on_arrival(jnp.sum(tok * tok, axis=1), "dp", 0)
    row_scale = lax.rsqrt(squares / D + EPS)
    normed = (tok * norm_gain).astype(jnp.bfloat16)
    own_rows = old_state.shape[0]
    outputs = []
    for partial_weight in weights:
        product = jnp.dot(normed, partial_weight, preferred_element_type=jnp.float32)
        outputs.append(lax.optimization_barrier(product.astype(jnp.bfloat16)).astype(jnp.float32))
    summed = summed_on_arrival_2(jnp.concatenate(outputs, axis=1).astype(jnp.bfloat16), "dp", 0)
    stored = lax.optimization_barrier((row_scale[:, None] * summed).astype(jnp.bfloat16)).astype(
        jnp.float32
    )
    heads_dev = old_state.shape[1]
    widths = [weight.shape[1] for weight in weights]
    offsets = [0, widths[0], widths[0] + widths[1], widths[0] + widths[1] + widths[2]]
    pieces = [
        stored[:, offsets[n] : offsets[n] + widths[n]].reshape(own_rows, heads_dev, -1)
        for n in range(4)
    ]
    query = jax.nn.silu(pieces[0]) * DK ** (-0.5)
    forget_pre, value, gate_pre = (pieces[1], pieces[2], pieces[3])
    floor_heads = floor_rate.reshape(heads_dev, -1)
    forget = floor_heads + (1.0 - floor_heads) * jax.nn.sigmoid(forget_pre)
    key_in = (1.0 - floor_heads) * jax.nn.sigmoid(-forget_pre)
    updated = old_state * forget[..., None] + key_in[..., None] * value[:, :, None, :]
    read = jnp.einsum("bhk,bhkv->bhv", query, updated)
    read = read * lax.rsqrt(jnp.mean(read * read, axis=-1, keepdims=True) + EPS) * head_gain
    gated = (read * jax.nn.silu(gate_pre)).reshape(own_rows, -1).astype(jnp.bfloat16)
    partial_update = jnp.dot(
        gather_directly(gated, "dp", 0), w_output, preferred_element_type=jnp.float32
    )
    share = summed_on_arrival_2(partial_update.astype(jnp.bfloat16), "tp", 0)
    share_rows = share.shape[0]
    own_tok = lax.dynamic_slice_in_dim(tok, lax.axis_index("tp") * share_rows, share_rows, 0)
    fresh = (own_tok + share).astype(jnp.bfloat16)
    result = gather_directly(fresh, "tp", 0)
    return (result, updated)


def per_device(
    tokens, norm_gain, w_query, w_forget, w_value, w_gate, floor_rate, head_gain, w_output, state
):
    current = tokens
    states = []
    for layer_index in range(2):
        weights = (
            w_query[layer_index],
            w_forget[layer_index],
            w_value[layer_index],
            w_gate[layer_index],
        )
        current, updated = mixer_layer(
            current,
            norm_gain[layer_index],
            weights,
            floor_rate[layer_index],
            head_gain[layer_index],
            w_output[layer_index],
            state[layer_index],
        )
        states.append(updated)
    return (current, jnp.stack(states, axis=0))


def solution(mesh):
    in_specs = (
        P(None, "dp"),
        P(None, "dp"),
        P(None, "dp", "tp"),
        P(None, "dp", "tp"),
        P(None, "dp", "tp"),
        P(None, "dp", "tp"),
        P(None, "tp"),
        P(),
        P(None, "tp", "dp"),
        P(None, "dp", "tp", None, None),
    )
    out_specs = (P(None, "dp"), P(None, "dp", "tp", None, None))
    return jax.shard_map(
        per_device, mesh=mesh, in_specs=in_specs, out_specs=out_specs, check_vma=False
    )
```

profile of v0, /device:TPU:1, one launch (start us, length us, event | category | flops | bytes accessed | tf_op | source)
XLA Modules:
  0.0 139.1 jit_solution(4645404352190889821)
XLA Ops:
  0.7 1.2 multiply_reduce_fusion.1
  2.5 10.0 %all-to-all-start = ((f32[16,1,16]{2,1,0:T(1,128)}), f32[16,1,16]{2,1,0:T(1,128)S(1)}, u32[]{:S(2)}, u32[]{:S(2)}) async-start(f32[16,1,16]{2,1,0:T(1,128)} %all_to_all.36), calls=%async_computation | async-start | bytes 16384 | tf_op jit(solution)/shard_map/all_to_all | solution.py:21
  12.5 0.8 fusion.36
  13.3 1.1 convolution_convert_fusion.8
  14.4 1.1 convolution_convert_fusion.7
  15.5 1.1 convolution_convert_fusion.6
  16.6 1.1 convolution_convert_fusion.9
  17.7 0.7 pad_maximum_fusion.1
  18.4 1.1 all-to-all-done
  19.5 6.3 %all-to-all-start.1 = ((bf16[16,16,512]{2,1,0:T(8,128)(2,1)}), bf16[16,16,512]{2,1,0:T(8,128)(2,1)S(1)}, u32[]{:S(2)}, u32[]{:S(2)}) async-start(bf16[16,16,512]{2,1,0:T(8,128)(2,1)} %pad_maximum_fusion.1), calls=%async_computation.1 | async-start | bytes 524288 | tf_op jit(solution)/shard_map/all_to_all | solution.py:27
  25.9 11.5 %all-to-all-done.1 = bf16[16,16,512]{2,1,0:T(8,128)(2,1)S(1)} async-done(((bf16[16,16,512]{2,1,0:T(8,128)(2,1)}), bf16[16,16,512]{2,1,0:T(8,128)(2,1)S(1)}, u32[]{:S(2)}, u32[]{:S(2)}) %all-to-all-start.1) | async-done | bytes 262176 | tf_op jit(solution)/shard_map/all_to_all | solution.py:27
  37.6 0.7 fusion.4
  38.5 10.6 %all_to_all.58 = bf16[16,16,128]{2,1,0:T(8,128)(2,1)S(1)} all-to-all(bf16[16,16,128]{2,1,0:T(8,128)(2,1)S(1)} %broadcast_in_dim.8), channel_id=1, replica_groups=mesh['tp'=16,'dp'=16] {'dp'}, dimensions={0} | all-to-all | bytes 131072 | tf_op jit(solution)/shard_map/all_to_all | solution.py:33
  49.1 0.8 convolution_convert_fusion.1
  49.9 6.8 %all-to-all-start.3 = ((bf16[16,16,256]{2,1,0:T(8,128)(2,1)}), bf16[16,16,256]{2,1,0:T(8,128)(2,1)S(1)}, u32[]{:S(2)}, u32[]{:S(2)}) async-start(bf16[16,16,256]{2,1,0:T(8,128)(2,1)} %bitcast.20), calls=%async_computation.3 | async-start | bytes 262144 | tf_op jit(solution)/shard_map/all_to_all | solution.py:27
  56.7 6.8 %all-to-all-done.3 = bf16[16,16,256]{2,1,0:T(8,128)(2,1)S(1)} async-done(((bf16[16,16,256]{2,1,0:T(8,128)(2,1)}), bf16[16,16,256]{2,1,0:T(8,128)(2,1)S(1)}, u32[]{:S(2)}, u32[]{:S(2)}) %all-to-all-start.3) | async-done | bytes 131104 | tf_op jit(solution)/shard_map/all_to_all | solution.py:27
  63.6 9.9 %all_to_all.59 = bf16[16,16,256]{2,1,0:T(8,128)(2,1)S(1)} all-to-all(bf16[16,16,256]{2,1,0:T(8,128)(2,1)S(1)} %broadcast_in_dim.9), channel_id=1, replica_groups=mesh['tp'=16,'dp'=16] {'tp'}, dimensions={0} | all-to-all | bytes 262144 | tf_op jit(solution)/shard_map/all_to_all | solution.py:33
  74.9 6.0 %all-to-all-start.5 = ((f32[16,1,16]{2,1,0:T(1,128)}), f32[16,1,16]{2,1,0:T(1,128)S(1)}, u32[]{:S(2)}, u32[]{:S(2)}) async-start(f32[16,1,16]{2,1,0:T(1,128)} %bitcast.22), calls=%async_computation.5 | async-start | bytes 16384 | tf_op jit(solution)/shard_map/all_to_all | solution.py:21
  80.9 0.7 pad_maximum_fusion.2
  81.6 6.3 %all-to-all-done.5 = f32[16,1,16]{2,1,0:T(1,128)S(1)} async-done(((f32[16,1,16]{2,1,0:T(1,128)}), f32[16,1,16]{2,1,0:T(1,128)S(1)}, u32[]{:S(2)}, u32[]{:S(2)}) %all-to-all-start.5) | async-done | bytes 1056 | tf_op jit(solution)/shard_map/all_to_all | solution.py:21
  87.9 4.0 %all-to-all-start.6 = ((bf16[16,16,512]{2,1,0:T(8,128)(2,1)}), bf16[16,16,512]{2,1,0:T(8,128)(2,1)S(1)}, u32[]{:S(2)}, u32[]{:S(2)}) async-start(bf16[16,16,512]{2,1,0:T(8,128)(2,1)} %pad_maximum_fusion.2), calls=%async_computation.6 | async-start | bytes 524288 | tf_op jit(solution)/shard_map/all_to_all | solution.py:27
  92.0 11.7 %all-to-all-done.6 = bf16[16,16,512]{2,1,0:T(8,128)(2,1)S(1)} async-done(((bf16[16,16,512]{2,1,0:T(8,128)(2,1)}), bf16[16,16,512]{2,1,0:T(8,128)(2,1)S(1)}, u32[]{:S(2)}, u32[]{:S(2)}) %all-to-all-start.6) | async-done | bytes 262176 | tf_op jit(solution)/shard_map/all_to_all | solution.py:27
  103.8 0.7 fusion.1
  105.4 3.4 %all-to-all-start.7 = ((bf16[16,16,128]{2,1,0:T(8,128)(2,1)}), bf16[16,16,128]{2,1,0:T(8,128)(2,1)S(1)}, u32[]{:S(2)}, u32[]{:S(2)}) async-start(bf16[16,16,128]{2,1,0:T(8,128)(2,1)} %broadcast_in_dim.10), calls=%async_computation.7 | async-start | bytes 131072 | tf_op jit(solution)/shard_map/all_to_all | solution.py:33
  108.9 7.1 %all-to-all-done.7 = bf16[16,16,128]{2,1,0:T(8,128)(2,1)S(1)} async-done(((bf16[16,16,128]{2,1,0:T(8,128)(2,1)}), bf16[16,16,128]{2,1,0:T(8,128)(2,1)S(1)}, u32[]{:S(2)}, u32[]{:S(2)}) %all-to-all-start.7) | async-done | bytes 65568 | tf_op jit(solution)/shard_map/all_to_all | solution.py:33
  116.0 0.8 convolution_convert_fusion
  116.8 3.5 %all-to-all-start.8 = ((bf16[16,16,256]{2,1,0:T(8,128)(2,1)}), bf16[16,16,256]{2,1,0:T(8,128)(2,1)S(1)}, u32[]{:S(2)}, u32[]{:S(2)}) async-start(bf16[16,16,256]{2,1,0:T(8,128)(2,1)} %bitcast.43), calls=%async_computation.8 | async-start | bytes 262144 | tf_op jit(solution)/shard_map/all_to_all | solution.py:27
  120.3 2.7 %multiply_add_fusion.1 = (f32[1,16,1,128,128]{4,3,2,1,0:T(8,128)S(1)}, f32[1,16,1,128,128]{4,3,2,1,0:T(8,128)}) fusion(f32[2,16,1,128,128]{4,3,2,1,0:T(8,128)S(1)} %copy-done, f32[16,128]{1,0:T(8,128)S(1)} %slice.106, f32[16,128]{1,0:T(8,128)} %copy-done.4, f32[16,128]{1,0:T(8,128)} %copy-done.3, f32[16,128]{1,0:T(8,128)S(1)} %slice.110, ...), kind=kLoop, calls=%fused_computation.18 | loop fusion | flops 1572864 | bytes 4243456 | tf_op jit(solution)/shard_map/add | solution.py:73
  123.0 4.4 %all-to-all-done.8 = bf16[16,16,256]{2,1,0:T(8,128)(2,1)S(1)} async-done(((bf16[16,16,256]{2,1,0:T(8,128)(2,1)}), bf16[16,16,256]{2,1,0:T(8,128)(2,1)S(1)}, u32[]{:S(2)}, u32[]{:S(2)}) %all-to-all-start.8) | async-done | bytes 131104 | tf_op jit(solution)/shard_map/all_to_all | solution.py:27
  128.1 3.5 %all-to-all-start.9 = ((bf16[16,16,256]{2,1,0:T(8,128)(2,1)}), bf16[16,16,256]{2,1,0:T(8,128)(2,1)S(1)}, u32[]{:S(2)}, u32[]{:S(2)}) async-start(bf16[16,16,256]{2,1,0:T(8,128)(2,1)} %broadcast_in_dim.11), calls=%async_computation.9 | async-start | bytes 262144 | tf_op jit(solution)/shard_map/all_to_all | solution.py:33
  131.6 2.7 %pad_maximum_fusion = f32[2,16,1,128,128]{4,3,2,1,0:T(8,128)} fusion(f32[1,16,1,128,128]{4,3,2,1,0:T(8,128)} %get-tuple-element.3, f32[1,16,1,128,128]{4,3,2,1,0:T(8,128)S(1)} %get-tuple-element.2), kind=kLoop, calls=%fused_computation | loop fusion | flops 524288 | bytes 4194304 | tf_op jit(solution)/shard_map/stack | solution.py:110
  134.4 4.1 %all-to-all-done.9 = bf16[16,16,256]{2,1,0:T(8,128)(2,1)S(1)} async-done(((bf16[16,16,256]{2,1,0:T(8,128)(2,1)}), bf16[16,16,256]{2,1,0:T(8,128)(2,1)S(1)}, u32[]{:S(2)}, u32[]{:S(2)}) %all-to-all-start.9) | async-done | bytes 131104 | tf_op jit(solution)/shard_map/all_to_all | solution.py:33
  (65 shorter events, 5.0 us)
Async XLA Ops:
  0.6 25.2 %copy-start.12 = (f32[2,128]{1,0:T(2,128)S(1)}, f32[2,128]{1,0:T(2,128)}, u32[]{:S(2)}) copy-start(f32[2,128]{1,0:T(2,128)} %param.17) | copy-start | bytes 3076
  0.6 25.2 %copy-start.11 = (f32[2,128]{1,0:T(2,128)S(1)}, f32[2,128]{1,0:T(2,128)}, u32[]{:S(2)}) copy-start(f32[2,128]{1,0:T(2,128)} %param.16) | copy-start | bytes 3076
  0.7 36.9 %copy-start = (f32[2,16,1,128,128]{4,3,2,1,0:T(8,128)S(1)}, f32[2,16,1,128,128]{4,3,2,1,0:T(8,128)}, u32[]{:S(2)}) copy-start(f32[2,16,1,128,128]{4,3,2,1,0:T(8,128)} %param.19) | copy-start | bytes 6291460
  0.7 48.4 %copy-start.2 = (bf16[2,128,256]{2,1,0:T(8,128)(2,1)S(1)}, bf16[2,128,256]{2,1,0:T(8,128)(2,1)}, u32[]{:S(2)}) copy-start(bf16[2,128,256]{2,1,0:T(8,128)(2,1)} %param.18) | copy-start | bytes 393220
  2.5 16.9 %all-to-all-start = ((f32[16,1,16]{2,1,0:T(1,128)}), f32[16,1,16]{2,1,0:T(1,128)S(1)}, u32[]{:S(2)}, u32[]{:S(2)}) async-start(f32[16,1,16]{2,1,0:T(1,128)} %all_to_all.36), calls=%async_computation | async-start | bytes 16384 | tf_op jit(solution)/shard_map/all_to_all | solution.py:21
  14.3 42.3 %copy-start.1 = (bf16[256,256]{1,0:T(8,128)(2,1)S(1)}, bf16[256,256]{1,0:T(8,128)(2,1)}, u32[]{:S(2)}) copy-start(bf16[256,256]{1,0:T(8,128)(2,1)} %param.10) | copy-start | bytes 393220
  18.4 55.8 %copy-start.7 = (bf16[2,256,128]{2,1,0:T(8,128)(2,1)S(1)}, bf16[2,256,128]{2,1,0:T(8,128)(2,1)}, u32[]{:S(2)}) copy-start(bf16[2,256,128]{2,1,0:T(8,128)(2,1)} %param.15) | copy-start | bytes 393220
  18.4 56.0 %copy-start.8 = (bf16[2,256,128]{2,1,0:T(8,128)(2,1)S(1)}, bf16[2,256,128]{2,1,0:T(8,128)(2,1)}, u32[]{:S(2)}) copy-start(bf16[2,256,128]{2,1,0:T(8,128)(2,1)} %param.14) | copy-start | bytes 393220
  19.5 17.9 %all-to-all-start.1 = ((bf16[16,16,512]{2,1,0:T(8,128)(2,1)}), bf16[16,16,512]{2,1,0:T(8,128)(2,1)S(1)}, u32[]{:S(2)}, u32[]{:S(2)}) async-start(bf16[16,16,512]{2,1,0:T(8,128)(2,1)} %pad_maximum_fusion.1), calls=%async_computation.1 | async-start | bytes 524288 | tf_op jit(solution)/shard_map/all_to_all | solution.py:27
  25.8 48.8 %copy-start.9 = (bf16[2,256,128]{2,1,0:T(8,128)(2,1)S(1)}, bf16[2,256,128]{2,1,0:T(8,128)(2,1)}, u32[]{:S(2)}) copy-start(bf16[2,256,128]{2,1,0:T(8,128)(2,1)} %param.13) | copy-start | bytes 393220
  37.4 37.4 %copy-start.10 = (bf16[2,256,128]{2,1,0:T(8,128)(2,1)S(1)}, bf16[2,256,128]{2,1,0:T(8,128)(2,1)}, u32[]{:S(2)}) copy-start(bf16[2,256,128]{2,1,0:T(8,128)(2,1)} %param.12) | copy-start | bytes 393220
  37.5 19.1 %copy-start.3 = (f32[16,128]{1,0:T(8,128)}, f32[16,128]{1,0:T(8,128)S(1)}, u32[]{:S(2)}) copy-start(f32[16,128]{1,0:T(8,128)S(1)} %get-tuple-element.8) | copy-start | bytes 24580
  37.5 19.1 %copy-start.4 = (f32[16,128]{1,0:T(8,128)}, f32[16,128]{1,0:T(8,128)S(1)}, u32[]{:S(2)}) copy-start(f32[16,128]{1,0:T(8,128)S(1)} %get-tuple-element.9) | copy-start | bytes 24580
  49.9 13.6 %all-to-all-start.3 = ((bf16[16,16,256]{2,1,0:T(8,128)(2,1)}), bf16[16,16,256]{2,1,0:T(8,128)(2,1)S(1)}, u32[]{:S(2)}, u32[]{:S(2)}) async-start(bf16[16,16,256]{2,1,0:T(8,128)(2,1)} %bitcast.20), calls=%async_computation.3 | async-start | bytes 262144 | tf_op jit(solution)/shard_map/all_to_all | solution.py:27
  74.9 13.0 %all-to-all-start.5 = ((f32[16,1,16]{2,1,0:T(1,128)}), f32[16,1,16]{2,1,0:T(1,128)S(1)}, u32[]{:S(2)}, u32[]{:S(2)}) async-start(f32[16,1,16]{2,1,0:T(1,128)} %bitcast.22), calls=%async_computation.5 | async-start | bytes 16384 | tf_op jit(solution)/shard_map/all_to_all | solution.py:21
  87.9 15.7 %all-to-all-start.6 = ((bf16[16,16,512]{2,1,0:T(8,128)(2,1)}), bf16[16,16,512]{2,1,0:T(8,128)(2,1)S(1)}, u32[]{:S(2)}, u32[]{:S(2)}) async-start(bf16[16,16,512]{2,1,0:T(8,128)(2,1)} %pad_maximum_fusion.2), calls=%async_computation.6 | async-start | bytes 524288 | tf_op jit(solution)/shard_map/all_to_all | solution.py:27
  103.8 1.6 %copy-start.5 = (f32[16,128]{1,0:T(8,128)}, f32[16,128]{1,0:T(8,128)S(1)}, u32[]{:S(2)}) copy-start(f32[16,128]{1,0:T(8,128)S(1)} %get-tuple-element.6) | copy-start | bytes 24580
  103.8 1.6 %copy-start.6 = (f32[16,128]{1,0:T(8,128)}, f32[16,128]{1,0:T(8,128)S(1)}, u32[]{:S(2)}) copy-start(f32[16,128]{1,0:T(8,128)S(1)} %get-tuple-element.7) | copy-start | bytes 24580
  105.4 10.5 %all-to-all-start.7 = ((bf16[16,16,128]{2,1,0:T(8,128)(2,1)}), bf16[16,16,128]{2,1,0:T(8,128)(2,1)S(1)}, u32[]{:S(2)}, u32[]{:S(2)}) async-start(bf16[16,16,128]{2,1,0:T(8,128)(2,1)} %broadcast_in_dim.10), calls=%async_computation.7 | async-start | bytes 131072 | tf_op jit(solution)/shard_map/all_to_all | solution.py:33
  116.8 10.6 %all-to-all-start.8 = ((bf16[16,16,256]{2,1,0:T(8,128)(2,1)}), bf16[16,16,256]{2,1,0:T(8,128)(2,1)S(1)}, u32[]{:S(2)}, u32[]{:S(2)}) async-start(bf16[16,16,256]{2,1,0:T(8,128)(2,1)} %bitcast.43), calls=%async_computation.8 | async-start | bytes 262144 | tf_op jit(solution)/shard_map/all_to_all | solution.py:27
  128.1 10.4 %all-to-all-start.9 = ((bf16[16,16,256]{2,1,0:T(8,128)(2,1)}), bf16[16,16,256]{2,1,0:T(8,128)(2,1)S(1)}, u32[]{:S(2)}, u32[]{:S(2)}) async-start(bf16[16,16,256]{2,1,0:T(8,128)(2,1)} %broadcast_in_dim.11), calls=%async_computation.9 | async-start | bytes 262144 | tf_op jit(solution)/shard_map/all_to_all | solution.py:33
where the time goes:
time: 140 us; the launch traced here: 139 us
  waiting for transfers between devices  52.9 us (38%)
  starting transfers between devices  43.4 us (31%)
  blocking collectives  20.5 us (15%)
  other arithmetic  9.67 us (7%)
  matrix products  8.13 us (6%)
  local copies, waits for them, and re-layouts  3.54 us (3%)
    all_to_all x4, waiting for transfers between devices, summed_on_arrival_2(): lax.all_to_all(parts, axis, split_axis=0, concat_axis=0, tiled=True)  34.4 us
    all_to_all x4, starting transfers between devices, summed_on_arrival_2(): lax.all_to_all(parts, axis, split_axis=0, concat_axis=0, tiled=True)  20.6 us
    all_to_all x2, blocking collectives, from_everyone(): return lax.all_to_all(copies, axis, split_axis=0, concat_axis=0, tiled=True)  20.5 us
    all_to_all x2, starting transfers between devices, summed_on_arrival(): lax.all_to_all(parts, axis, split_axis=0, concat_axis=0, tiled=True)  15.9 us
    all_to_all x2, waiting for transfers between devices, from_everyone(): return lax.all_to_all(copies, axis, split_axis=0, concat_axis=0, tiled=True)  11.2 us
    all_to_all x2, waiting for transfers between devices, summed_on_arrival(): lax.all_to_all(parts, axis, split_axis=0, concat_axis=0, tiled=True)  7.33 us
    all_to_all x2, starting transfers between devices, from_everyone(): return lax.all_to_all(copies, axis, split_axis=0, concat_axis=0, tiled=True)  6.91 us
    dot_general x8, matrix products, mixer_layer(): jnp.dot(normed, partial_weight, preferred_element_type=jnp.float32)  5.04 us
  transfers between devices with their start and end apart: 8, of which 8 were waited for; matrix products, arithmetic and copies ran while one was open for 9% of the time, Pallas kernels for 0%

commit v1 on v0

v1 whole, which is shorter than its diff:
```python
import functools

import jax
import jax.numpy as jnp
from jax import lax
from jax.experimental import pallas as pl
from jax.experimental.pallas import tpu as pltpu
from jax.sharding import PartitionSpec as P

D = 4096
DK = 128
EPS = 1e-06
MESH = pl.DeviceIdType.MESH
F32 = jnp.float32
BF16 = jnp.bfloat16

Z_ORDER = (0, 1, 7, 2, 6, 3, 5, 4)
C_GROUPS = ((0, 6), (6, 10), (10, 16))
E_GROUPS = (0, 2, 3, 1)


def gray(v):
    return v + v // 2 - 2 * (v // 3)


def tp_slot(dy, dx):
    return (dx % 2) * 8 + (dx // 2) * 4 + gray(dy)


def z_slot(dz, rel):
    return 2 * Z_ORDER.index(dz) + rel


def z_slot_traced(dz, rel):
    pos = jnp.where(dz <= 4, 2 * dz - jnp.minimum(dz, 1), 16 - 2 * dz)
    return 2 * pos + rel


def kernel(
    tok_in,
    gain_in,
    wq_in,
    wf_in,
    wv_in,
    wg_in,
    floor_in,
    hgain_in,
    wout_in,
    state_in,
    mixed_out,
    state_out,
    cur,
    gain,
    w,
    floor,
    hgain,
    wout,
    old,
    part,
    pair_in,
    pair,
    sums_in,
    sq,
    sq_pair_in,
    sq_pair,
    sq_in,
    gat,
    upd,
    upd_in,
    final,
    load_sem,
    tok_sem,
    a1_send,
    a1_recv,
    s1_send,
    s1_recv,
    a2_send,
    a2_recv,
    s2_send,
    s2_recv,
    c_send,
    c_recv,
    d_send,
    d_recv,
    e_send,
    e_recv,
):
    h = lax.axis_index("tp")
    d = lax.axis_index("dp")
    y, x = h // 4, h % 4
    z, core = d // 2, d % 2
    e = (x + core) % 2
    partner = {"dp": 2 * z + 1 - core}

    barrier = pltpu.get_barrier_semaphore()
    for k in range(1, 16):
        pl.semaphore_signal(barrier, inc=1, device_id={"tp": (h + k) % 16}, device_id_type=MESH)
        pl.semaphore_signal(barrier, inc=1, device_id={"dp": (d + k) % 16}, device_id_type=MESH)

    toks = []
    for dy in range(4):
        for dx in range(4):
            rows = ((y + dy) % 4) * 4 + (x + dx) % 4
            copy = pltpu.make_async_copy(
                tok_in.at[pl.ds(rows * 16, 16), :], cur.at[0, tp_slot(dy, dx)], tok_sem
            )
            copy.start()
    tok_all = pltpu.make_async_copy(cur.at[0], cur.at[0], tok_sem)

    loads = {}

    def load(name, src, dst):
        loads[name] = pltpu.make_async_copy(src, dst, load_sem.at[len(loads)])
        loads[name].start()

    weights = (wq_in, wf_in, wv_in, wg_in)
    load("gain", gain_in, gain)
    for n in range(4):
        load(("w", 0, n), weights[n].at[0], w.at[0, :, pl.ds(128 * n, 128)])
    load("floor", floor_in, floor)
    load("hgain", hgain_in, hgain)
    load(("state", 0), state_in.at[0, :, 0], old.at[0])
    load(("wout", 0), wout_in.at[0], wout.at[0])
    for n in range(4):
        load(("w", 1, n), weights[n].at[1], w.at[1, :, pl.ds(128 * n, 128)])
    load(("state", 1), state_in.at[1, :, 0], old.at[1])
    load(("wout", 1), wout_in.at[1], wout.at[1])

    own = pl.multiple_of(8 * e, 8)
    other = pl.multiple_of(8 - 8 * e, 8)
    self_dy = ((2 * z + core) // 4 - y + 4) % 4
    self_dx = ((2 * z + core) % 4 - x + 4) % 4
    self_slot = (self_dx // 2) * 4 + gray(self_dy)
    up_dz = (h // 2 - z + 8) % 8
    up_rel = (h % 2 + core) % 2
    up_slot = z_slot_traced(up_dz, up_rel)

    def remote(src, dst, send, recv, device):
        return pltpu.make_async_remote_copy(
            src_ref=src,
            dst_ref=dst,
            send_sem=send,
            recv_sem=recv,
            device_id=device,
            device_id_type=MESH,
        )

    def wait_bytes(ref, sem):
        pltpu.make_async_copy(ref, ref, sem).wait()

    def project(l, first, count):
        rows = cur[l, pl.ds(first, count)].astype(F32).reshape(16 * count, 256)
        normed = (rows * gain[l : l + 1, :]).astype(BF16)
        product = jnp.dot(normed, w[l], preferred_element_type=F32)
        part[l, pl.ds(first, count)] = product.astype(BF16).reshape(count, 16, 512)

    def squares(l):
        ones = jnp.ones((8, 256), BF16)
        for c in range(2):
            rows = cur[l, 8 * c : 8 * c + 8].astype(F32).reshape(128, 256)
            square = rows * rows
            high = square.astype(BF16)
            low = (square - high.astype(F32)).astype(BF16)
            dims = (((1,), (1,)), ((), ()))
            total = lax.dot_general(ones, high, dims, preferred_element_type=F32)
            total += lax.dot_general(ones, low, dims, preferred_element_type=F32)
            sq[l, c] = total[:1]

    def send_pair(l, half):
        remote(
            part.at[l, pl.ds(other + 4 * half, 4)],
            pair_in.at[l, pl.ds(4 * half, 4)],
            a1_send.at[l, half],
            a1_recv.at[l, half],
            partner,
        ).start()

    def send_squares(l):
        remote(sq.at[l, 1 - e], sq_pair_in.at[l], s1_send.at[l], s1_recv.at[l], partner).start()

    for l in range(2):
        if l == 0:
            tok_all.wait()
            loads["gain"].wait()
            for n in range(4):
                loads["w", 0, n].wait()
            project(0, other, 8)
            squares(0)
            pl.semaphore_wait(barrier, 30)
            send_squares(0)
            send_pair(0, 0)
            send_pair(0, 1)
            project(0, own, 8)
        else:
            for n in range(4):
                loads["w", 1, n].wait()
            for group in E_GROUPS:
                arrived = 3 if group == 0 else 4
                wait_bytes(cur.at[1, pl.ds(0, arrived)], e_recv.at[0, group])
                project(1, 4 * group, 4)

                @pl.when(e != group // 2)
                def _():
                    send_pair(1, group % 2)

            squares(1)
            send_squares(1)

        wait_bytes(sq_pair_in.at[l], s1_recv.at[l])
        sq_pair[l] = sq[l, e] + sq_pair_in[l]
        for k in range(1, 8):
            remote(
                sq_pair.at[l],
                sq_in.at[l, 8 - k],
                s2_send.at[l],
                s2_recv.at[l],
                {"dp": (d + 2 * k) % 16},
            ).start()
        for half in range(2):
            wait_bytes(pair_in.at[l, pl.ds(0, 4)], a1_recv.at[l, half])
            mine = part[l, pl.ds(own + 4 * half, 4)].astype(F32)
            theirs = pair_in[l, 4 * half : 4 * half + 4].astype(F32)
            pair[l, 4 * half : 4 * half + 4] = (mine + theirs).astype(BF16)
            for i in range(4):
                block = ((y + gray(i)) % 4) * 4 + (x + 2 * half + e) % 4
                to_z = block // 2

                @pl.when(to_z != z)
                def _():
                    remote(
                        pair.at[l, 4 * half + i],
                        sums_in.at[l, (z - to_z + 8) % 8],
                        a2_send.at[l],
                        a2_recv.at[l],
                        {"dp": 2 * to_z + core},
                    ).start()

        wait_bytes(sq_in.at[l, pl.ds(0, 7)], s2_recv.at[l])
        row = sq_pair[l]
        for k in range(1, 8):
            row = row + sq_in[l, k]
        lanes = lax.broadcasted_iota(jnp.int32, (16, 128), 1)
        rows = lax.broadcasted_iota(jnp.int32, (16, 128), 0)
        picked = jnp.where(lanes == rows + 16 * self_slot, jnp.broadcast_to(row, (16, 128)), 0.0)
        row_scale = lax.rsqrt(jnp.sum(picked, axis=1, keepdims=True) / D + EPS)
        if l == 0:
            loads["floor"].wait()
            loads["hgain"].wait()
        loads["state", l].wait()
        wait_bytes(sums_in.at[l, pl.ds(0, 7)], a2_recv.at[l])
        total = pair[l, self_slot].astype(F32)
        for k in range(1, 8):
            total = total + sums_in[l, k].astype(F32)
        stored = (row_scale * total).astype(BF16).astype(F32)
        query_pre, forget_pre = stored[:, :128], stored[:, 128:256]
        value, gate_pre = stored[:, 256:384], stored[:, 384:]
        query = jax.nn.silu(query_pre) * DK ** (-0.5)
        low = floor[l : l + 1, :]
        forget = low + (1.0 - low) * jax.nn.sigmoid(forget_pre)
        key_in = (1.0 - low) * jax.nn.sigmoid(-forget_pre)
        scaled = (query * forget).T
        reads = []
        for b in range(16):
            reads.append(jnp.sum(old[l, b] * scaled[:, b : b + 1], axis=0, keepdims=True))
        read = jnp.concatenate(reads, axis=0)
        read = read + jnp.sum(query * key_in, axis=1, keepdims=True) * value
        read = read * lax.rsqrt(jnp.mean(read * read, axis=1, keepdims=True) + EPS)
        gated = read * hgain[l : l + 1, :] * jax.nn.silu(gate_pre)
        gat[l, 0] = gated.astype(BF16)

        for dz in reversed(Z_ORDER):
            for rel in (1, 0):
                if dz == 0 and rel == 0:
                    continue
                slot = z_slot((8 - dz) % 8, rel)
                to_core = core if rel == 0 else 1 - core
                group = [slot >= first and slot < last for first, last in C_GROUPS].index(True)
                remote(
                    gat.at[l, 0],
                    gat.at[l, slot],
                    c_send.at[l],
                    c_recv.at[l, group],
                    {"dp": 2 * ((z + dz) % 8) + to_core},
                ).start()

        forget_t, key_t = forget.T, key_in.T
        for b in range(16):
            kept = old[l, b] * forget_t[:, b : b + 1]
            state_out[l, b, 0] = kept + key_t[:, b : b + 1] * value[b : b + 1, :]

        loads["wout", l].wait()
        for group, (first, last) in enumerate(C_GROUPS):
            arrived = last - first - (1 if group == 0 else 0)
            wait_bytes(gat.at[l, pl.ds(0, arrived)], c_recv.at[l, group])
            rows = gat[l, first:last].reshape(16 * (last - first), 128)
            product = jnp.dot(rows, wout[l], preferred_element_type=F32)
            upd[l, first:last] = product.astype(BF16).reshape(last - first, 16, 256)
            for slot in range(first, last):
                dz, rel = Z_ORDER[slot // 2], slot % 2
                to_core = core if rel == 0 else 1 - core
                owner = 2 * ((z + dz) % 8) + to_core
                dy = (y - owner // 4 + 4) % 4
                dx = (x - owner % 4 + 4) % 4

                @pl.when(owner != h)
                def _():
                    remote(
                        upd.at[l, slot],
                        upd_in.at[l, tp_slot(dy, dx)],
                        d_send.at[l],
                        d_recv.at[l],
                        {"tp": owner},
                    ).start()

        wait_bytes(upd_in.at[l, pl.ds(0, 15)], d_recv.at[l])
        share = upd[l, up_slot].astype(F32)
        for s in range(1, 16):
            share = share + upd_in[l, s].astype(F32)
        fresh = (cur[l, 0].astype(F32) + share).astype(BF16)

        if l == 0:
            cur[1, 0] = fresh
        else:
            final[h] = fresh
        offsets = [(dy, dx) for dy in range(4) for dx in range(4) if dy or dx]
        near = (0, 1, 2, 1)
        offsets.sort(key=lambda o: -near[o[0]] - near[o[1]])
        for dy, dx in offsets:
            to = ((y + dy) % 4) * 4 + (x + dx) % 4
            slot = tp_slot((4 - dy) % 4, (4 - dx) % 4)
            if l == 0:
                src, dst, recv = cur.at[1, 0], cur.at[1, slot], e_recv.at[0, slot // 4]
            else:
                src, dst, recv = final.at[h], final.at[h], e_recv.at[1, 0]
            remote(src, dst, e_send.at[l], recv, {"tp": to}).start()

    for l in range(2):
        wait_bytes(sq_pair_in.at[l], s1_send.at[l])
        wait_bytes(sq_in.at[l, pl.ds(0, 7)], s2_send.at[l])
        for half in range(2):
            wait_bytes(pair_in.at[l, pl.ds(0, 4)], a1_send.at[l, half])
        wait_bytes(sums_in.at[l, pl.ds(0, 7)], a2_send.at[l])
        wait_bytes(gat.at[l, pl.ds(0, 15)], c_send.at[l])
        wait_bytes(upd_in.at[l, pl.ds(0, 15)], d_send.at[l])
        wait_bytes(cur.at[0, pl.ds(0, 15)], e_send.at[l])
    wait_bytes(final.at[pl.ds(0, 15)], e_recv.at[1, 0])
    mixed_out[...] = final[...].reshape(256, 256)


def per_device(*args):
    any_spec = pl.BlockSpec(memory_space=pl.ANY)
    vmem_spec = pl.BlockSpec(memory_space=pltpu.VMEM)
    dma = pltpu.SemaphoreType.DMA
    return pl.pallas_call(
        kernel,
        out_shape=(
            jax.ShapeDtypeStruct((256, 256), BF16),
            jax.ShapeDtypeStruct((2, 16, 1, 128, 128), F32),
        ),
        in_specs=[any_spec] * 10,
        out_specs=(vmem_spec, vmem_spec),
        scratch_shapes=[
            pltpu.VMEM((2, 16, 16, 256), BF16),
            pltpu.VMEM((2, 256), F32),
            pltpu.VMEM((2, 256, 512), BF16),
            pltpu.VMEM((2, 128), F32),
            pltpu.VMEM((2, 128), F32),
            pltpu.VMEM((2, 128, 256), BF16),
            pltpu.VMEM((2, 16, 128, 128), F32),
            pltpu.VMEM((2, 16, 16, 512), BF16),
            pltpu.VMEM((2, 8, 16, 512), BF16),
            pltpu.VMEM((2, 8, 16, 512), BF16),
            pltpu.VMEM((2, 8, 16, 512), BF16),
            pltpu.VMEM((2, 2, 1, 128), F32),
            pltpu.VMEM((2, 1, 128), F32),
            pltpu.VMEM((2, 1, 128), F32),
            pltpu.VMEM((2, 8, 1, 128), F32),
            pltpu.VMEM((2, 16, 16, 128), BF16),
            pltpu.VMEM((2, 16, 16, 256), BF16),
            pltpu.VMEM((2, 16, 16, 256), BF16),
            pltpu.VMEM((16, 16, 256), BF16),
            dma((17,)),
            dma,
            dma((2, 2)),
            dma((2, 2)),
            dma((2,)),
            dma((2,)),
            dma((2,)),
            dma((2,)),
            dma((2,)),
            dma((2,)),
            dma((2,)),
            dma((2, 3)),
            dma((2,)),
            dma((2,)),
            dma((2,)),
            dma((2, 4)),
        ],
        compiler_params=pltpu.CompilerParams(collective_id=0, has_side_effects=True),
    )(*args)


def solution(mesh):
    in_specs = (
        P(None, "dp"),
        P(None, "dp"),
        P(None, "dp", "tp"),
        P(None, "dp", "tp"),
        P(None, "dp", "tp"),
        P(None, "dp", "tp"),
        P(None, "tp"),
        P(),
        P(None, "tp", "dp"),
        P(None, "dp", "tp", None, None),
    )
    out_specs = (P(None, "dp"), P(None, "dp", "tp", None, None))
    return jax.shard_map(
        per_device, mesh=mesh, in_specs=in_specs, out_specs=out_specs, check_vma=False
    )
```

time: 140 us -> 60.2 us (0.43)
  Pallas kernels: 0 us -> 54.7 us
  waiting for transfers between devices: 52.9 us -> 0 us
  starting transfers between devices: 43.4 us -> 0 us
  blocking collectives: 20.5 us -> 0 us
  other arithmetic: 9.67 us -> 0 us
  matrix products: 8.13 us -> 0 us
    pallas_call x0 -> x1, Pallas kernels: none -> 54.7 us  [per_device(): pl.pallas_call(kernel, out_shape=(jax.ShapeDtypeStruct((256, 256), BF16),...]
    all_to_all x8 -> x0, waiting for transfers between devices: 52.9 us -> none  [the longest x4 34.4 us: summed_on_arrival_2(): lax.all_to_all(parts, axis, split_axis=0, concat_axis=0, tiled=True)]
    all_to_all x8 -> x0, starting transfers between devices: 43.4 us -> none  [the longest x4 20.6 us: summed_on_arrival_2(): lax.all_to_all(parts, axis, split_axis=0, concat_axis=0, tiled=True)]
    all_to_all x2 -> x0, blocking collectives: 20.5 us -> none  [from_everyone(): return lax.all_to_all(copies, axis, split_axis=0, concat_axis=0, tiled=True)]
    dot_general x12 -> x0, matrix products: 8.13 us -> none  [the longest x8 5.04 us: mixer_layer(): jnp.dot(normed, partial_weight, preferred_element_type=jnp.float32)]
    unnamed x27 -> x2, local copies, waits for them, and re-layouts: 0.72 us -> 4.7 us
    add x4 -> x0, other arithmetic: 2.77 us -> none  [the longest x1 2.73 us: mixer_layer(): old_state * forget[..., None] + key_in[..., None] * value[:, :, None, :]]
    another operation x1 -> x0, other arithmetic: 2.73 us -> none  [per_device(): return (current, jnp.stack(states, axis=0))]
  transfers between devices with their start and end apart: 8 -> 0, of which waited for: 8 -> 0; matrix products, arithmetic and copies ran while one was open for 9% -> 0% of each run, Pallas kernels for 0% -> 0%
where the time goes in v1:
time: 60.2 us; the launch traced here: 60.1 us
  Pallas kernels  54.7 us (91%)
  local copies, waits for them, and re-layouts  4.7 us (8%)
  between operations  0.64 us (1%)
    pallas_call x1, Pallas kernels, per_device(): pl.pallas_call(kernel, out_shape=(jax.ShapeDtypeStruct((256, 256), BF16),...  54.7 us
    unnamed x2, local copies, waits for them, and re-layouts  4.7 us

profile of v1, /device:TPU:1, one launch (start us, length us, event | category | flops | bytes accessed | tf_op | source)
XLA Modules:
  0.0 60.1 jit_solution(2440270223587574753)
XLA Ops:
  0.6 54.7 %shard_map.113 = (bf16[256,256]{1,0:T(8,128)(2,1)}, f32[2,16,1,128,128]{4,3,2,1,0:T(8,128)}) custom-call(bf16[256,256]{1,0:T(8,128)(2,1)} %tok_in.1, f32[2,256]{1,0:T(2,128)} %gain_in.1, bf16[2,256,128]{2,1,0:T(8,128)(2,1)} %wq_in.1, bf16[2,256,128]{2,1,0:T(8,128)(2,1)} %wf_in.1, bf16[2,256,128]{2,1,0:T(8,128)(2,1)} %wv_in.1, bf16[2,256,128]{2,1,0:T(8,128)(2,1)} %wg_in.1, ...), custom_call_target="tpu_custom_call" | custom-call | tf_op jit(solution)/shard_map/pallas_call | solution.py:354
  55.4 1.6 %copy.14 = bf16[256,256]{1,0:T(8,128)(2,1)} copy(bf16[256,256]{1,0:T(8,128)(2,1)} %get-tuple-element.4) | data formatting | bytes 262144
  56.9 3.1 %copy.15 = f32[2,16,1,128,128]{4,3,2,1,0:T(8,128)} copy(f32[2,16,1,128,128]{4,3,2,1,0:T(8,128)} %get-tuple-element.5) | data formatting | bytes 4194304

commit v2 on v1

--- a/solution.py
+++ b/solution.py
@@ -92,11 +92,6 @@
     e = (x + core) % 2
     partner = {"dp": 2 * z + 1 - core}
 
-    barrier = pltpu.get_barrier_semaphore()
-    for k in range(1, 16):
-        pl.semaphore_signal(barrier, inc=1, device_id={"tp": (h + k) % 16}, device_id_type=MESH)
-        pl.semaphore_signal(barrier, inc=1, device_id={"dp": (d + k) % 16}, device_id_type=MESH)
-
     toks = []
     for dy in range(4):
         for dx in range(4):
@@ -117,14 +112,10 @@
     load("gain", gain_in, gain)
     for n in range(4):
         load(("w", 0, n), weights[n].at[0], w.at[0, :, pl.ds(128 * n, 128)])
-    load("floor", floor_in, floor)
-    load("hgain", hgain_in, hgain)
-    load(("state", 0), state_in.at[0, :, 0], old.at[0])
-    load(("wout", 0), wout_in.at[0], wout.at[0])
-    for n in range(4):
-        load(("w", 1, n), weights[n].at[1], w.at[1, :, pl.ds(128 * n, 128)])
-    load(("state", 1), state_in.at[1, :, 0], old.at[1])
-    load(("wout", 1), wout_in.at[1], wout.at[1])
+    barrier = pltpu.get_barrier_semaphore()
+    for k in range(1, 16):
+        pl.semaphore_signal(barrier, inc=1, device_id={"tp": (h + k) % 16}, device_id_type=MESH)
+        pl.semaphore_signal(barrier, inc=1, device_id={"dp": (d + k) % 16}, device_id_type=MESH)
 
     own = pl.multiple_of(8 * e, 8)
     other = pl.multiple_of(8 - 8 * e, 8)
@@ -185,6 +176,14 @@
             for n in range(4):
                 loads["w", 0, n].wait()
             project(0, other, 8)
+            load("floor", floor_in, floor)
+            load("hgain", hgain_in, hgain)
+            load(("state", 0), state_in.at[0, :, 0], old.at[0])
+            load(("wout", 0), wout_in.at[0], wout.at[0])
+            for n in range(4):
+                load(("w", 1, n), weights[n].at[1], w.at[1, :, pl.ds(128 * n, 128)])
+            load(("state", 1), state_in.at[1, :, 0], old.at[1])
+            load(("wout", 1), wout_in.at[1], wout.at[1])
             squares(0)
             pl.semaphore_wait(barrier, 30)
             send_squares(0)
@@ -347,16 +346,26 @@
     mixed_out[...] = final[...].reshape(256, 256)
 
 
+def write_out(mixed, state, mixed_out, state_out, sem):
+    copies = [pltpu.make_async_copy(mixed, mixed_out, sem.at[8])]
+    for n in range(8):
+        part = state.at[n // 4, pl.ds(4 * (n % 4), 4)]
+        target = state_out.at[n // 4, pl.ds(4 * (n % 4), 4)]
+        copies.append(pltpu.make_async_copy(part, target, sem.at[n]))
+    for copy in copies:
+        copy.start()
+    for copy in copies:
+        copy.wait()
+
+
 def per_device(*args):
     any_spec = pl.BlockSpec(memory_space=pl.ANY)
     vmem_spec = pl.BlockSpec(memory_space=pltpu.VMEM)
     dma = pltpu.SemaphoreType.DMA
-    return pl.pallas_call(
+    shapes = ((256, 256), BF16), ((2, 16, 1, 128, 128), F32)
+    held = pl.pallas_call(
         kernel,
-        out_shape=(
-            jax.ShapeDtypeStruct((256, 256), BF16),
-            jax.ShapeDtypeStruct((2, 16, 1, 128, 128), F32),
-        ),
+        out_shape=tuple(pltpu.VMEM(shape, dtype) for shape, dtype in shapes),
         in_specs=[any_spec] * 10,
         out_specs=(vmem_spec, vmem_spec),
         scratch_shapes=[
@@ -398,6 +407,14 @@
         ],
         compiler_params=pltpu.CompilerParams(collective_id=0, has_side_effects=True),
     )(*args)
+    return pl.pallas_call(
+        write_out,
+        out_shape=tuple(jax.ShapeDtypeStruct(shape, dtype) for shape, dtype in shapes),
+        in_specs=[any_spec] * 2,
+        out_specs=[any_spec] * 2,
+        scratch_shapes=[dma((9,))],
+        compiler_params=pltpu.CompilerParams(vmem_limit_bytes=1 << 20),
+    )(*held)
 
 
 def solution(mesh):

time: 60.2 us -> 55.7 us (0.925)
  local copies, waits for them, and re-layouts: 4.7 us -> 0 us
    unnamed x2 -> x0, local copies, waits for them, and re-layouts: 4.7 us -> none
    pallas_call x1 -> x2, Pallas kernels: 54.7 us -> 55 us  [the longest x1 53.5 us: per_device(): pl.pallas_call(kernel, out_shape=tuple((pltpu.VMEM(shape, dtype) for shap...]
where the time goes in v2:
time: 55.7 us; the launch traced here: 55.6 us
  Pallas kernels  55 us (99%)
  between operations  0.64 us (1%)
    pallas_call x1, Pallas kernels, per_device(): pl.pallas_call(kernel, out_shape=tuple((pltpu.VMEM(shape, dtype) for shap...  53.5 us
    pallas_call x1, Pallas kernels, per_device(): pl.pallas_call(write_out, out_shape=tuple((jax.ShapeDtypeStruct(shape, dt...  1.43 us

profile of v2, /device:TPU:1, one launch (start us, length us, event | category | flops | bytes accessed | tf_op | source)
XLA Modules:
  0.0 55.6 jit_solution(10426735915796377106)
XLA Ops:
  0.6 53.5 %shard_map.113 = (bf16[256,256]{1,0:T(8,128)(2,1)S(1)}, f32[2,16,1,128,128]{4,3,2,1,0:T(8,128)S(1)}) custom-call(bf16[256,256]{1,0:T(8,128)(2,1)} %tok_in.1, f32[2,256]{1,0:T(2,128)} %gain_in.1, bf16[2,256,128]{2,1,0:T(8,128)(2,1)} %wq_in.1, bf16[2,256,128]{2,1,0:T(8,128)(2,1)} %wf_in.1, bf16[2,256,128]{2,1,0:T(8,128)(2,1)} %wv_in.1, ...), custom_call_target="tpu_custom_call" | custom-call | tf_op jit(solution)/shard_map/pallas_call | solution.py:366
  54.2 1.4 %shard_map.114 = (bf16[256,256]{1,0:T(8,128)(2,1)}, f32[2,16,1,128,128]{4,3,2,1,0:T(8,128)}) custom-call(bf16[256,256]{1,0:T(8,128)(2,1)S(1)} %get-tuple-element.4.mixed, f32[2,16,1,128,128]{4,3,2,1,0:T(8,128)S(1)} %get-tuple-element.5.state), custom_call_target="tpu_custom_call" | custom-call | tf_op jit(solution)/shard_map/pallas_call | solution.py:410

commit v3 on v2

--- a/solution.py
+++ b/solution.py
@@ -16,7 +16,6 @@
 
 Z_ORDER = (0, 1, 7, 2, 6, 3, 5, 4)
 C_GROUPS = ((0, 6), (6, 10), (10, 16))
-E_GROUPS = (0, 2, 3, 1)
 
 
 def gray(v):
@@ -50,8 +49,12 @@
     mixed_out,
     state_out,
     cur,
+    cur1,
+    held,
     gain,
-    w,
+    gain1,
+    w0,
+    w1,
     floor,
     hgain,
     wout,
@@ -74,6 +77,10 @@
     a1_recv,
     s1_send,
     s1_recv,
+    w1_send,
+    w1_recv,
+    g1_send,
+    g1_recv,
     a2_send,
     a2_recv,
     s2_send,
@@ -84,6 +91,8 @@
     d_recv,
     e_send,
     e_recv,
+    e_send_pair,
+    final_recv,
 ):
     h = lax.axis_index("tp")
     d = lax.axis_index("dp")
@@ -97,10 +106,10 @@
         for dx in range(4):
             rows = ((y + dy) % 4) * 4 + (x + dx) % 4
             copy = pltpu.make_async_copy(
-                tok_in.at[pl.ds(rows * 16, 16), :], cur.at[0, tp_slot(dy, dx)], tok_sem
+                tok_in.at[pl.ds(rows * 16, 16), :], cur.at[tp_slot(dy, dx)], tok_sem
             )
             copy.start()
-    tok_all = pltpu.make_async_copy(cur.at[0], cur.at[0], tok_sem)
+    tok_all = pltpu.make_async_copy(cur, cur, tok_sem)
 
     loads = {}
 
@@ -111,11 +120,14 @@
     weights = (wq_in, wf_in, wv_in, wg_in)
     load("gain", gain_in, gain)
     for n in range(4):
-        load(("w", 0, n), weights[n].at[0], w.at[0, :, pl.ds(128 * n, 128)])
+        load(("w", 0, n), weights[n].at[0], w0.at[:, pl.ds(128 * n, 128)])
     barrier = pltpu.get_barrier_semaphore()
     for k in range(1, 16):
-        pl.semaphore_signal(barrier, inc=1, device_id={"tp": (h + k) % 16}, device_id_type=MESH)
+        to = (h + k) % 16
         pl.semaphore_signal(barrier, inc=1, device_id={"dp": (d + k) % 16}, device_id_type=MESH)
+        pl.semaphore_signal(barrier, inc=1, device_id={"tp": to}, device_id_type=MESH)
+        across = {"tp": to, **partner}
+        pl.semaphore_signal(barrier, inc=1, device_id=across, device_id_type=MESH)
 
     own = pl.multiple_of(8 * e, 8)
     other = pl.multiple_of(8 - 8 * e, 8)
@@ -139,74 +151,37 @@
     def wait_bytes(ref, sem):
         pltpu.make_async_copy(ref, ref, sem).wait()
 
-    def project(l, first, count):
-        rows = cur[l, pl.ds(first, count)].astype(F32).reshape(16 * count, 256)
-        normed = (rows * gain[l : l + 1, :]).astype(BF16)
-        product = jnp.dot(normed, w[l], preferred_element_type=F32)
-        part[l, pl.ds(first, count)] = product.astype(BF16).reshape(count, 16, 512)
-
-    def squares(l):
-        ones = jnp.ones((8, 256), BF16)
-        for c in range(2):
-            rows = cur[l, 8 * c : 8 * c + 8].astype(F32).reshape(128, 256)
-            square = rows * rows
-            high = square.astype(BF16)
-            low = (square - high.astype(F32)).astype(BF16)
-            dims = (((1,), (1,)), ((), ()))
-            total = lax.dot_general(ones, high, dims, preferred_element_type=F32)
-            total += lax.dot_general(ones, low, dims, preferred_element_type=F32)
-            sq[l, c] = total[:1]
-
-    def send_pair(l, half):
-        remote(
-            part.at[l, pl.ds(other + 4 * half, 4)],
-            pair_in.at[l, pl.ds(4 * half, 4)],
-            a1_send.at[l, half],
-            a1_recv.at[l, half],
-            partner,
-        ).start()
-
-    def send_squares(l):
-        remote(sq.at[l, 1 - e], sq_pair_in.at[l], s1_send.at[l], s1_recv.at[l], partner).start()
-
-    for l in range(2):
-        if l == 0:
-            tok_all.wait()
-            loads["gain"].wait()
-            for n in range(4):
-                loads["w", 0, n].wait()
-            project(0, other, 8)
-            load("floor", floor_in, floor)
-            load("hgain", hgain_in, hgain)
-            load(("state", 0), state_in.at[0, :, 0], old.at[0])
-            load(("wout", 0), wout_in.at[0], wout.at[0])
-            for n in range(4):
-                load(("w", 1, n), weights[n].at[1], w.at[1, :, pl.ds(128 * n, 128)])
-            load(("state", 1), state_in.at[1, :, 0], old.at[1])
-            load(("wout", 1), wout_in.at[1], wout.at[1])
-            squares(0)
-            pl.semaphore_wait(barrier, 30)
-            send_squares(0)
-            send_pair(0, 0)
-            send_pair(0, 1)
-            project(0, own, 8)
-        else:
-            for n in range(4):
-                loads["w", 1, n].wait()
-            for group in E_GROUPS:
-                arrived = 3 if group == 0 else 4
-                wait_bytes(cur.at[1, pl.ds(0, arrived)], e_recv.at[0, group])
-                project(1, 4 * group, 4)
-
-                @pl.when(e != group // 2)
-                def _():
-                    send_pair(1, group % 2)
-
-            squares(1)
-            send_squares(1)
-
-        wait_bytes(sq_pair_in.at[l], s1_recv.at[l])
-        sq_pair[l] = sq[l, e] + sq_pair_in[l]
+    def project(first, count):
+        rows = cur[pl.ds(first, count)].astype(F32).reshape(16 * count, 256)
+        normed = (rows * gain[0:1, :]).astype(BF16)
+        product = jnp.dot(normed, w0[...], preferred_element_type=F32)
+        part[pl.ds(first, count)] = product.astype(BF16).reshape(count, 16, 512)
+
+    def squares(rows):
+        ones = jnp.ones((8, rows.shape[1]), BF16)
+        square = rows * rows
+        high = square.astype(BF16)
+        low = (square - high.astype(F32)).astype(BF16)
+        dims = (((1,), (1,)), ((), ()))
+        total = lax.dot_general(ones, high, dims, preferred_element_type=F32)
+        total += lax.dot_general(ones, low, dims, preferred_element_type=F32)
+        return total[:1]
+
+    def send_along_z(l, i):
+        block = ((y + gray(i % 4)) % 4) * 4 + (x + 2 * (i // 4) + e) % 4
+        to_z = block // 2
+
+        @pl.when(to_z != z)
+        def _():
+            remote(
+                pair.at[l, i],
+                sums_in.at[l, (z - to_z + 8) % 8],
+                a2_send.at[l],
+                a2_recv.at[l],
+                {"dp": 2 * to_z + core},
+            ).start()
+
+    def send_squares_along_z(l):
         for k in range(1, 8):
             remote(
                 sq_pair.at[l],
@@ -215,24 +190,59 @@
                 s2_recv.at[l],
                 {"dp": (d + 2 * k) % 16},
             ).start()
-        for half in range(2):
-            wait_bytes(pair_in.at[l, pl.ds(0, 4)], a1_recv.at[l, half])
-            mine = part[l, pl.ds(own + 4 * half, 4)].astype(F32)
-            theirs = pair_in[l, 4 * half : 4 * half + 4].astype(F32)
-            pair[l, 4 * half : 4 * half + 4] = (mine + theirs).astype(BF16)
-            for i in range(4):
-                block = ((y + gray(i)) % 4) * 4 + (x + 2 * half + e) % 4
-                to_z = block // 2
-
-                @pl.when(to_z != z)
-                def _():
-                    remote(
-                        pair.at[l, 4 * half + i],
-                        sums_in.at[l, (z - to_z + 8) % 8],
-                        a2_send.at[l],
-                        a2_recv.at[l],
-                        {"dp": 2 * to_z + core},
-                    ).start()
+
+    for l in range(2):
+        if l == 0:
+            tok_all.wait()
+            loads["gain"].wait()
+            for n in range(4):
+                loads["w", 0, n].wait()
+            project(other, 8)
+            load("floor", floor_in, floor)
+            load("hgain", hgain_in, hgain)
+            load(("state", 0), state_in.at[0, :, 0], old.at[0])
+            load(("wout", 0), wout_in.at[0], wout.at[0])
+            for n in range(4):
+                load(("w", 1, n), weights[n].at[1], w1.at[core, :, pl.ds(128 * n, 128)])
+            load(("state", 1), state_in.at[1, :, 0], old.at[1])
+            load(("wout", 1), wout_in.at[1], wout.at[1])
+            for c in range(2):
+                sq[c] = squares(cur[8 * c : 8 * c + 8].astype(F32).reshape(128, 256))
+            pl.semaphore_wait(barrier, 45)
+            remote(sq.at[1 - e], sq_pair_in, s1_send, s1_recv, partner).start()
+            for half in range(2):
+                remote(
+                    part.at[pl.ds(other + 4 * half, 4)],
+                    pair_in.at[pl.ds(4 * half, 4)],
+                    a1_send.at[half],
+                    a1_recv.at[half],
+                    partner,
+                ).start()
+            project(own, 8)
+            wait_bytes(sq_pair_in, s1_recv)
+            sq_pair[0] = sq[e] + sq_pair_in[...]
+            send_squares_along_z(0)
+            for half in range(2):
+                wait_bytes(pair_in.at[pl.ds(0, 4)], a1_recv.at[half])
+                mine = part[pl.ds(own + 4 * half, 4)].astype(F32)
+                theirs = pair_in[4 * half : 4 * half + 4].astype(F32)
+                pair[0, 4 * half : 4 * half + 4] = (mine + theirs).astype(BF16)
+                for i in range(4):
+                    send_along_z(0, 4 * half + i)
+        else:
+            wait_bytes(w1.at[0], w1_recv)
+            wait_bytes(gain1.at[0], g1_recv)
+            for half in range(2):
+                wait_bytes(cur1.at[pl.ds(0, 4)], e_recv.at[half])
+                rows = cur1[4 * half : 4 * half + 4].astype(F32).reshape(64, 512)
+                normed = [(rows[:, 256 * c : 256 * c + 256] * gain1[c]).astype(BF16) for c in range(2)]
+                product = jnp.dot(normed[0], w1[0], preferred_element_type=F32)
+                product += jnp.dot(normed[1], w1[1], preferred_element_type=F32)
+                pair[1, 4 * half : 4 * half + 4] = product.astype(BF16).reshape(4, 16, 512)
+                for i in range(4):
+                    send_along_z(1, 4 * half + i)
+            sq_pair[1] = squares(cur1[...].astype(F32).reshape(128, 512))
+            send_squares_along_z(1)
 
         wait_bytes(sq_in.at[l, pl.ds(0, 7)], s2_recv.at[l])
         row = sq_pair[l]
@@ -282,6 +292,13 @@
                     {"dp": 2 * ((z + dz) % 8) + to_core},
                 ).start()
 
+        if l == 0:
+            for n in range(4):
+                loads["w", 1, n].wait()
+            remote(w1.at[core], w1.at[core], w1_send, w1_recv, partner).start()
+            gain1[core] = gain[1:2, :]
+            remote(gain1.at[core], gain1.at[core], g1_send, g1_recv, partner).start()
+
         forget_t, key_t = forget.T, key_in.T
         for b in range(16):
             kept = old[l, b] * forget_t[:, b : b + 1]
@@ -315,34 +332,55 @@
         share = upd[l, up_slot].astype(F32)
         for s in range(1, 16):
             share = share + upd_in[l, s].astype(F32)
-        fresh = (cur[l, 0].astype(F32) + share).astype(BF16)
-
-        if l == 0:
-            cur[1, 0] = fresh
-        else:
-            final[h] = fresh
+        before = cur[0] if l == 0 else held[...]
+        fresh = (before.astype(F32) + share).astype(BF16)
+
         offsets = [(dy, dx) for dy in range(4) for dx in range(4) if dy or dx]
         near = (0, 1, 2, 1)
         offsets.sort(key=lambda o: -near[o[0]] - near[o[1]])
-        for dy, dx in offsets:
-            to = ((y + dy) % 4) * 4 + (x + dx) % 4
-            slot = tp_slot((4 - dy) % 4, (4 - dx) % 4)
-            if l == 0:
-                src, dst, recv = cur.at[1, 0], cur.at[1, slot], e_recv.at[0, slot // 4]
-            else:
-                src, dst, recv = final.at[h], final.at[h], e_recv.at[1, 0]
-            remote(src, dst, e_send.at[l], recv, {"tp": to}).start()
-
+        if l == 0:
+            held[...] = fresh
+            to_core = x % 2
+            for dy, dx in offsets:
+                to = ((y + dy) % 4) * 4 + (x + dx) % 4
+                slot = tp_slot((4 - dy) % 4, (4 - dx) % 4) % 8
+                remote(
+                    held,
+                    cur1.at[slot, :, pl.ds(256 * core, 256)],
+                    e_send.at[0],
+                    e_recv.at[slot // 4],
+                    {"tp": to, "dp": 2 * z + to_core},
+                ).start()
+            target = cur1.at[0, :, pl.ds(256 * core, 256)]
+
+            @pl.when(to_core == core)
+            def _():
+                pltpu.make_async_copy(held, target, e_recv.at[0]).start()
+
+            @pl.when(to_core != core)
+            def _():
+                remote(held, target, e_send_pair, e_recv.at[0], partner).start()
+                wait_bytes(held, e_send_pair)
+        else:
+            final[h] = fresh
+            for dy, dx in offsets:
+                to = ((y + dy) % 4) * 4 + (x + dx) % 4
+                remote(
+                    final.at[h], final.at[h], e_send.at[1], final_recv, {"tp": to}
+                ).start()
+
+    wait_bytes(sq_pair_in, s1_send)
+    for half in range(2):
+        wait_bytes(pair_in.at[pl.ds(0, 4)], a1_send.at[half])
+    wait_bytes(w1.at[0], w1_send)
+    wait_bytes(gain1.at[0], g1_send)
     for l in range(2):
-        wait_bytes(sq_pair_in.at[l], s1_send.at[l])
         wait_bytes(sq_in.at[l, pl.ds(0, 7)], s2_send.at[l])
-        for half in range(2):
-            wait_bytes(pair_in.at[l, pl.ds(0, 4)], a1_send.at[l, half])
         wait_bytes(sums_in.at[l, pl.ds(0, 7)], a2_send.at[l])
         wait_bytes(gat.at[l, pl.ds(0, 15)], c_send.at[l])
         wait_bytes(upd_in.at[l, pl.ds(0, 15)], d_send.at[l])
-        wait_bytes(cur.at[0, pl.ds(0, 15)], e_send.at[l])
-    wait_bytes(final.at[pl.ds(0, 15)], e_recv.at[1, 0])
+        wait_bytes(cur.at[pl.ds(0, 15)], e_send.at[l])
+    wait_bytes(final.at[pl.ds(0, 15)], final_recv)
     mixed_out[...] = final[...].reshape(256, 256)
 
 
@@ -369,19 +407,23 @@
         in_specs=[any_spec] * 10,
         out_specs=(vmem_spec, vmem_spec),
         scratch_shapes=[
-            pltpu.VMEM((2, 16, 16, 256), BF16),
+            pltpu.VMEM((16, 16, 256), BF16),
+            pltpu.VMEM((8, 16, 512), BF16),
+            pltpu.VMEM((16, 256), BF16),
             pltpu.VMEM((2, 256), F32),
+            pltpu.VMEM((2, 1, 256), F32),
+            pltpu.VMEM((256, 512), BF16),
             pltpu.VMEM((2, 256, 512), BF16),
             pltpu.VMEM((2, 128), F32),
             pltpu.VMEM((2, 128), F32),
             pltpu.VMEM((2, 128, 256), BF16),
             pltpu.VMEM((2, 16, 128, 128), F32),
-            pltpu.VMEM((2, 16, 16, 512), BF16),
+            pltpu.VMEM((16, 16, 512), BF16),
+            pltpu.VMEM((8, 16, 512), BF16),
             pltpu.VMEM((2, 8, 16, 512), BF16),
             pltpu.VMEM((2, 8, 16, 512), BF16),
-            pltpu.VMEM((2, 8, 16, 512), BF16),
-            pltpu.VMEM((2, 2, 1, 128), F32),
             pltpu.VMEM((2, 1, 128), F32),
+            pltpu.VMEM((1, 128), F32),
             pltpu.VMEM((2, 1, 128), F32),
             pltpu.VMEM((2, 8, 1, 128), F32),
             pltpu.VMEM((2, 16, 16, 128), BF16),
@@ -390,10 +432,14 @@
             pltpu.VMEM((16, 16, 256), BF16),
             dma((17,)),
             dma,
-            dma((2, 2)),
-            dma((2, 2)),
-            dma((2,)),
-            dma((2,)),
+            dma((2,)),
+            dma((2,)),
+            dma,
+            dma,
+            dma,
+            dma,
+            dma,
+            dma,
             dma((2,)),
             dma((2,)),
             dma((2,)),
@@ -403,7 +449,9 @@
             dma((2,)),
             dma((2,)),
             dma((2,)),
-            dma((2, 4)),
+            dma((2,)),
+            dma,
+            dma,
         ],
         compiler_params=pltpu.CompilerParams(collective_id=0, has_side_effects=True),
     )(*args)

time: 55.7 us -> 55 us (0.987)
  Pallas kernels: 55 us -> 54.2 us
    pallas_call x1, Pallas kernels: 53.5 us -> 52.7 us  [per_device(): pl.pallas_call(kernel, out_shape=tuple((pltpu.VMEM(shape, dtype) for shap...]
where the time goes in v3:
time: 55 us; the launch traced here: 54.8 us
  Pallas kernels  54.2 us (99%)
  between operations  0.64 us (1%)
    pallas_call x1, Pallas kernels, per_device(): pl.pallas_call(kernel, out_shape=tuple((pltpu.VMEM(shape, dtype) for shap...  52.7 us
    pallas_call x1, Pallas kernels, per_device(): pl.pallas_call(write_out, out_shape=tuple((jax.ShapeDtypeStruct(shape, dt...  1.43 us

profile of v3, /device:TPU:1, one launch (start us, length us, event | category | flops | bytes accessed | tf_op | source)
XLA Modules:
  0.0 54.8 jit_solution(10037095915590904121)
XLA Ops:
  0.6 52.7 %shard_map.113 = (bf16[256,256]{1,0:T(8,128)(2,1)S(1)}, f32[2,16,1,128,128]{4,3,2,1,0:T(8,128)S(1)}) custom-call(bf16[256,256]{1,0:T(8,128)(2,1)} %tok_in.1, f32[2,256]{1,0:T(2,128)} %gain_in.1, bf16[2,256,128]{2,1,0:T(8,128)(2,1)} %wq_in.1, bf16[2,256,128]{2,1,0:T(8,128)(2,1)} %wf_in.1, bf16[2,256,128]{2,1,0:T(8,128)(2,1)} %wv_in.1, ...), custom_call_target="tpu_custom_call" | custom-call | tf_op jit(solution)/shard_map/pallas_call | solution.py:404
  53.4 1.4 %shard_map.114 = (bf16[256,256]{1,0:T(8,128)(2,1)}, f32[2,16,1,128,128]{4,3,2,1,0:T(8,128)}) custom-call(bf16[256,256]{1,0:T(8,128)(2,1)S(1)} %get-tuple-element.4.mixed, f32[2,16,1,128,128]{4,3,2,1,0:T(8,128)S(1)} %get-tuple-element.5.state), custom_call_target="tpu_custom_call" | custom-call | tf_op jit(solution)/shard_map/pallas_call | solution.py:458

commit v4 on v3

--- a/solution.py
+++ b/solution.py
@@ -14,8 +14,8 @@
 F32 = jnp.float32
 BF16 = jnp.bfloat16
 
-Z_ORDER = (0, 1, 7, 2, 6, 3, 5, 4)
-C_GROUPS = ((0, 6), (6, 10), (10, 16))
+Z_FAR = (4, 3, 5, 2, 6, 1, 7, 0)
+TP_GROUPS = (0, 2, 3, 1)
 
 
 def gray(v):
@@ -24,15 +24,6 @@
 
 def tp_slot(dy, dx):
     return (dx % 2) * 8 + (dx // 2) * 4 + gray(dy)
-
-
-def z_slot(dz, rel):
-    return 2 * Z_ORDER.index(dz) + rel
-
-
-def z_slot_traced(dz, rel):
-    pos = jnp.where(dz <= 4, 2 * dz - jnp.minimum(dz, 1), 16 - 2 * dz)
-    return 2 * pos + rel
 
 
 def kernel(
@@ -68,8 +59,7 @@
     sq_pair,
     sq_in,
     gat,
-    upd,
-    upd_in,
+    gat_in,
     final,
     load_sem,
     tok_sem,
@@ -87,8 +77,8 @@
     s2_recv,
     c_send,
     c_recv,
-    d_send,
-    d_recv,
+    o_send,
+    o_recv,
     e_send,
     e_recv,
     e_send_pair,
@@ -128,15 +118,26 @@
         pl.semaphore_signal(barrier, inc=1, device_id={"tp": to}, device_id_type=MESH)
         across = {"tp": to, **partner}
         pl.semaphore_signal(barrier, inc=1, device_id=across, device_id_type=MESH)
+        away = {"tp": to, "dp": h}
+        pl.semaphore_signal(barrier, inc=1, device_id=away, device_id_type=MESH)
+
+    @pl.when(h != d)
+    def _():
+        pl.semaphore_signal(barrier, inc=1, device_id={"dp": h}, device_id_type=MESH)
+
 
     own = pl.multiple_of(8 * e, 8)
     other = pl.multiple_of(8 - 8 * e, 8)
     self_dy = ((2 * z + core) // 4 - y + 4) % 4
     self_dx = ((2 * z + core) % 4 - x + 4) % 4
     self_slot = (self_dx // 2) * 4 + gray(self_dy)
-    up_dz = (h // 2 - z + 8) % 8
-    up_rel = (h % 2 + core) % 2
-    up_slot = z_slot_traced(up_dz, up_rel)
+    own_slot = tp_slot((y - d // 4 + 4) % 4, (x - d % 4 + 4) % 4)
+    near = (0, 1, 2, 1)
+    offsets = [(dy, dx) for dy in range(4) for dx in range(4) if dy or dx]
+    offsets.sort(key=lambda o: -near[o[0]] - near[o[1]])
+    peers = [
+        (((y + dy) % 4) * 4 + (x + dx) % 4, tp_slot((4 - dy) % 4, (4 - dx) % 4)) for dy, dx in offsets
+    ]
 
     def remote(src, dst, send, recv, device):
         return pltpu.make_async_remote_copy(
@@ -189,6 +190,13 @@
                 s2_send.at[l],
                 s2_recv.at[l],
                 {"dp": (d + 2 * k) % 16},
+            ).start()
+
+    def gather_weights(l):
+        loads["wout", l].wait()
+        for to, slot in peers:
+            remote(
+                wout.at[l, 0], wout.at[l, slot], o_send.at[l], o_recv.at[l], {"tp": to}
             ).start()
 
     for l in range(2):
@@ -201,14 +209,14 @@
             load("floor", floor_in, floor)
             load("hgain", hgain_in, hgain)
             load(("state", 0), state_in.at[0, :, 0], old.at[0])
-            load(("wout", 0), wout_in.at[0], wout.at[0])
+            load(("wout", 0), wout_in.at[0], wout.at[0, 0])
             for n in range(4):
                 load(("w", 1, n), weights[n].at[1], w1.at[core, :, pl.ds(128 * n, 128)])
             load(("state", 1), state_in.at[1, :, 0], old.at[1])
-            load(("wout", 1), wout_in.at[1], wout.at[1])
+            load(("wout", 1), wout_in.at[1], wout.at[1, 0])
             for c in range(2):
                 sq[c] = squares(cur[8 * c : 8 * c + 8].astype(F32).reshape(128, 256))
-            pl.semaphore_wait(barrier, 45)
+            pl.semaphore_wait(barrier, jnp.where(h == d, 60, 61))
             remote(sq.at[1 - e], sq_pair_in, s1_send, s1_recv, partner).start()
             for half in range(2):
                 remote(
@@ -229,6 +237,7 @@
                 pair[0, 4 * half : 4 * half + 4] = (mine + theirs).astype(BF16)
                 for i in range(4):
                     send_along_z(0, 4 * half + i)
+            gather_weights(0)
         else:
             wait_bytes(w1.at[0], w1_recv)
             wait_bytes(gain1.at[0], g1_recv)
@@ -275,22 +284,23 @@
         read = read + jnp.sum(query * key_in, axis=1, keepdims=True) * value
         read = read * lax.rsqrt(jnp.mean(read * read, axis=1, keepdims=True) + EPS)
         gated = read * hgain[l : l + 1, :] * jax.nn.silu(gate_pre)
-        gat[l, 0] = gated.astype(BF16)
-
-        for dz in reversed(Z_ORDER):
-            for rel in (1, 0):
-                if dz == 0 and rel == 0:
-                    continue
-                slot = z_slot((8 - dz) % 8, rel)
-                to_core = core if rel == 0 else 1 - core
-                group = [slot >= first and slot < last for first, last in C_GROUPS].index(True)
-                remote(
-                    gat.at[l, 0],
-                    gat.at[l, slot],
-                    c_send.at[l],
-                    c_recv.at[l, group],
-                    {"dp": 2 * ((z + dz) % 8) + to_core},
-                ).start()
+        gat[l] = gated.astype(BF16)
+
+        landing = gat_in.at[l, own_slot]
+        recv = c_recv.at[l, own_slot // 4]
+        for dz in Z_FAR:
+            for other_core in (1, 0):
+                to = 2 * ((z + dz) % 8) + (core + other_core) % 2
+
+                @pl.when((h != d) | (to != d))
+                def _():
+                    remote(
+                        gat.at[l], landing, c_send.at[l], recv, {"tp": d, "dp": to}
+                    ).start()
+
+        @pl.when(h == d)
+        def _():
+            pltpu.make_async_copy(gat.at[l], landing, recv).start()
 
         if l == 0:
             for n in range(4):
@@ -304,46 +314,22 @@
             kept = old[l, b] * forget_t[:, b : b + 1]
             state_out[l, b, 0] = kept + key_t[:, b : b + 1] * value[b : b + 1, :]
 
-        loads["wout", l].wait()
-        for group, (first, last) in enumerate(C_GROUPS):
-            arrived = last - first - (1 if group == 0 else 0)
-            wait_bytes(gat.at[l, pl.ds(0, arrived)], c_recv.at[l, group])
-            rows = gat[l, first:last].reshape(16 * (last - first), 128)
-            product = jnp.dot(rows, wout[l], preferred_element_type=F32)
-            upd[l, first:last] = product.astype(BF16).reshape(last - first, 16, 256)
-            for slot in range(first, last):
-                dz, rel = Z_ORDER[slot // 2], slot % 2
-                to_core = core if rel == 0 else 1 - core
-                owner = 2 * ((z + dz) % 8) + to_core
-                dy = (y - owner // 4 + 4) % 4
-                dx = (x - owner % 4 + 4) % 4
-
-                @pl.when(owner != h)
-                def _():
-                    remote(
-                        upd.at[l, slot],
-                        upd_in.at[l, tp_slot(dy, dx)],
-                        d_send.at[l],
-                        d_recv.at[l],
-                        {"tp": owner},
-                    ).start()
-
-        wait_bytes(upd_in.at[l, pl.ds(0, 15)], d_recv.at[l])
-        share = upd[l, up_slot].astype(F32)
-        for s in range(1, 16):
-            share = share + upd_in[l, s].astype(F32)
+        wait_bytes(wout.at[l, pl.ds(0, 15)], o_recv.at[l])
+        share = jnp.zeros((16, 256), F32)
+        for group in TP_GROUPS:
+            wait_bytes(gat_in.at[l, pl.ds(0, 4)], c_recv.at[l, group])
+            heads = [gat_in[l, 4 * group + i] for i in range(4)]
+            rows = jnp.concatenate(heads, axis=1)
+            columns = wout[l, 4 * group : 4 * group + 4].reshape(512, 256)
+            share += jnp.dot(rows, columns, preferred_element_type=F32)
         before = cur[0] if l == 0 else held[...]
         fresh = (before.astype(F32) + share).astype(BF16)
 
-        offsets = [(dy, dx) for dy in range(4) for dx in range(4) if dy or dx]
-        near = (0, 1, 2, 1)
-        offsets.sort(key=lambda o: -near[o[0]] - near[o[1]])
         if l == 0:
             held[...] = fresh
             to_core = x % 2
-            for dy, dx in offsets:
-                to = ((y + dy) % 4) * 4 + (x + dx) % 4
-                slot = tp_slot((4 - dy) % 4, (4 - dx) % 4) % 8
+            for to, tp_slot_there in peers:
+                slot = tp_slot_there % 8
                 remote(
                     held,
                     cur1.at[slot, :, pl.ds(256 * core, 256)],
@@ -361,10 +347,11 @@
             def _():
                 remote(held, target, e_send_pair, e_recv.at[0], partner).start()
                 wait_bytes(held, e_send_pair)
+
+            gather_weights(1)
         else:
             final[h] = fresh
-            for dy, dx in offsets:
-                to = ((y + dy) % 4) * 4 + (x + dx) % 4
+            for to, _ in peers:
                 remote(
                     final.at[h], final.at[h], e_send.at[1], final_recv, {"tp": to}
                 ).start()
@@ -377,8 +364,16 @@
     for l in range(2):
         wait_bytes(sq_in.at[l, pl.ds(0, 7)], s2_send.at[l])
         wait_bytes(sums_in.at[l, pl.ds(0, 7)], a2_send.at[l])
-        wait_bytes(gat.at[l, pl.ds(0, 15)], c_send.at[l])
-        wait_bytes(upd_in.at[l, pl.ds(0, 15)], d_send.at[l])
+        wait_bytes(wout.at[l, pl.ds(0, 15)], o_send.at[l])
+
+        @pl.when(h == d)
+        def _():
+            wait_bytes(gat_in.at[l, pl.ds(0, 15)], c_send.at[l])
+
+        @pl.when(h != d)
+        def _():
+            wait_bytes(gat_in.at[l], c_send.at[l])
+
         wait_bytes(cur.at[pl.ds(0, 15)], e_send.at[l])
     wait_bytes(final.at[pl.ds(0, 15)], final_recv)
     mixed_out[...] = final[...].reshape(256, 256)
@@ -416,7 +411,7 @@
             pltpu.VMEM((2, 256, 512), BF16),
             pltpu.VMEM((2, 128), F32),
             pltpu.VMEM((2, 128), F32),
-            pltpu.VMEM((2, 128, 256), BF16),
+            pltpu.VMEM((2, 16, 128, 256), BF16),
             pltpu.VMEM((2, 16, 128, 128), F32),
             pltpu.VMEM((16, 16, 512), BF16),
             pltpu.VMEM((8, 16, 512), BF16),
@@ -426,9 +421,8 @@
             pltpu.VMEM((1, 128), F32),
             pltpu.VMEM((2, 1, 128), F32),
             pltpu.VMEM((2, 8, 1, 128), F32),
+            pltpu.VMEM((2, 16, 128), BF16),
             pltpu.VMEM((2, 16, 16, 128), BF16),
-            pltpu.VMEM((2, 16, 16, 256), BF16),
-            pltpu.VMEM((2, 16, 16, 256), BF16),
             pltpu.VMEM((16, 16, 256), BF16),
             dma((17,)),
             dma,
@@ -445,7 +439,7 @@
             dma((2,)),
             dma((2,)),
             dma((2,)),
-            dma((2, 3)),
+            dma((2, 4)),
             dma((2,)),
             dma((2,)),
             dma((2,)),

time: 55 us -> 60.8 us (1.11)
  Pallas kernels: 54.2 us -> 60 us
    pallas_call x1, Pallas kernels: 52.7 us -> 58.6 us  [per_device(): pl.pallas_call(kernel, out_shape=tuple((pltpu.VMEM(shape, dtype) for shap...]
where the time goes in v4:
time: 60.8 us; the launch traced here: 60.6 us
  Pallas kernels  60 us (99%)
  between operations  0.64 us (1%)
    pallas_call x1, Pallas kernels, per_device(): pl.pallas_call(kernel, out_shape=tuple((pltpu.VMEM(shape, dtype) for shap...  58.6 us
    pallas_call x1, Pallas kernels, per_device(): pl.pallas_call(write_out, out_shape=tuple((jax.ShapeDtypeStruct(shape, dt...  1.43 us

profile of v4, /device:TPU:1, one launch (start us, length us, event | category | flops | bytes accessed | tf_op | source)
XLA Modules:
  0.0 60.6 jit_solution(4629020415660661518)
XLA Ops:
  0.6 58.6 %shard_map.113 = (bf16[256,256]{1,0:T(8,128)(2,1)S(1)}, f32[2,16,1,128,128]{4,3,2,1,0:T(8,128)S(1)}) custom-call(bf16[256,256]{1,0:T(8,128)(2,1)} %tok_in.1, f32[2,256]{1,0:T(2,128)} %gain_in.1, bf16[2,256,128]{2,1,0:T(8,128)(2,1)} %wq_in.1, bf16[2,256,128]{2,1,0:T(8,128)(2,1)} %wf_in.1, bf16[2,256,128]{2,1,0:T(8,128)(2,1)} %wv_in.1, ...), custom_call_target="tpu_custom_call" | custom-call | tf_op jit(solution)/shard_map/pallas_call | solution.py:399
  59.2 1.4 %shard_map.114 = (bf16[256,256]{1,0:T(8,128)(2,1)}, f32[2,16,1,128,128]{4,3,2,1,0:T(8,128)}) custom-call(bf16[256,256]{1,0:T(8,128)(2,1)S(1)} %get-tuple-element.4.mixed, f32[2,16,1,128,128]{4,3,2,1,0:T(8,128)S(1)} %get-tuple-element.5.state), custom_call_target="tpu_custom_call" | custom-call | tf_op jit(solution)/shard_map/pallas_call | solution.py:452

commit v5 on v4

--- a/solution.py
+++ b/solution.py
@@ -77,8 +77,10 @@
     s2_recv,
     c_send,
     c_recv,
-    o_send,
-    o_recv,
+    ox_send,
+    ox_recv,
+    oy_send,
+    oy_recv,
     e_send,
     e_recv,
     e_send_pair,
@@ -192,12 +194,32 @@
                 {"dp": (d + 2 * k) % 16},
             ).start()
 
-    def gather_weights(l):
+    def along_x(dx):
+        return {"tp": y * 4 + (x + dx) % 4}
+
+    def along_y(dy):
+        return {"tp": ((y + dy) % 4) * 4 + x}
+
+    upper, lower = pl.ds(0, 64), pl.ds(64, 64)
+
+    def gather_first(l):
         loads["wout", l].wait()
-        for to, slot in peers:
-            remote(
-                wout.at[l, 0], wout.at[l, slot], o_send.at[l], o_recv.at[l], {"tp": to}
-            ).start()
+        for n in (2, 1, 3):
+            there = tp_slot(0, 4 - n) // 4
+            src, dst = wout.at[l, 0, 0, upper], wout.at[l, there, 0, upper]
+            remote(src, dst, ox_send.at[l, 0], ox_recv.at[l, 0], along_x(n)).start()
+            src, dst = wout.at[l, 0, 0, lower], wout.at[l, 0, gray(4 - n), lower]
+            remote(src, dst, oy_send.at[l, 0], oy_recv.at[l, 0], along_y(n)).start()
+
+    def gather_second(l):
+        wait_bytes(wout.at[l, 0, pl.ds(0, 3), upper], ox_recv.at[l, 0])
+        wait_bytes(wout.at[l, 0, pl.ds(0, 3), lower], oy_recv.at[l, 0])
+        for n in (2, 1, 3):
+            src, dst = wout.at[l, :, 0, upper], wout.at[l, :, gray(4 - n), upper]
+            remote(src, dst, oy_send.at[l, 1], oy_recv.at[l, 1], along_y(n)).start()
+            there = tp_slot(0, 4 - n) // 4
+            src, dst = wout.at[l, 0, :, lower], wout.at[l, there, :, lower]
+            remote(src, dst, ox_send.at[l, 1], ox_recv.at[l, 1], along_x(n)).start()
 
     for l in range(2):
         if l == 0:
@@ -209,11 +231,11 @@
             load("floor", floor_in, floor)
             load("hgain", hgain_in, hgain)
             load(("state", 0), state_in.at[0, :, 0], old.at[0])
-            load(("wout", 0), wout_in.at[0], wout.at[0, 0])
+            load(("wout", 0), wout_in.at[0], wout.at[0, 0, 0])
             for n in range(4):
                 load(("w", 1, n), weights[n].at[1], w1.at[core, :, pl.ds(128 * n, 128)])
             load(("state", 1), state_in.at[1, :, 0], old.at[1])
-            load(("wout", 1), wout_in.at[1], wout.at[1, 0])
+            load(("wout", 1), wout_in.at[1], wout.at[1, 0, 0])
             for c in range(2):
                 sq[c] = squares(cur[8 * c : 8 * c + 8].astype(F32).reshape(128, 256))
             pl.semaphore_wait(barrier, jnp.where(h == d, 60, 61))
@@ -226,6 +248,7 @@
                     a1_recv.at[half],
                     partner,
                 ).start()
+            gather_first(0)
             project(own, 8)
             wait_bytes(sq_pair_in, s1_recv)
             sq_pair[0] = sq[e] + sq_pair_in[...]
@@ -237,12 +260,14 @@
                 pair[0, 4 * half : 4 * half + 4] = (mine + theirs).astype(BF16)
                 for i in range(4):
                     send_along_z(0, 4 * half + i)
-            gather_weights(0)
         else:
             wait_bytes(w1.at[0], w1_recv)
             wait_bytes(gain1.at[0], g1_recv)
             for half in range(2):
                 wait_bytes(cur1.at[pl.ds(0, 4)], e_recv.at[half])
+                if half == 1:
+                    sq_pair[1] = squares(cur1[...].astype(F32).reshape(128, 512))
+                    send_squares_along_z(1)
                 rows = cur1[4 * half : 4 * half + 4].astype(F32).reshape(64, 512)
                 normed = [(rows[:, 256 * c : 256 * c + 256] * gain1[c]).astype(BF16) for c in range(2)]
                 product = jnp.dot(normed[0], w1[0], preferred_element_type=F32)
@@ -250,8 +275,7 @@
                 pair[1, 4 * half : 4 * half + 4] = product.astype(BF16).reshape(4, 16, 512)
                 for i in range(4):
                     send_along_z(1, 4 * half + i)
-            sq_pair[1] = squares(cur1[...].astype(F32).reshape(128, 512))
-            send_squares_along_z(1)
+        gather_second(l)
 
         wait_bytes(sq_in.at[l, pl.ds(0, 7)], s2_recv.at[l])
         row = sq_pair[l]
@@ -314,13 +338,17 @@
             kept = old[l, b] * forget_t[:, b : b + 1]
             state_out[l, b, 0] = kept + key_t[:, b : b + 1] * value[b : b + 1, :]
 
-        wait_bytes(wout.at[l, pl.ds(0, 15)], o_recv.at[l])
+        if l == 0:
+            gather_first(1)
+
+        wait_bytes(wout.at[l, pl.ds(0, 3), :, upper], oy_recv.at[l, 1])
+        wait_bytes(wout.at[l, pl.ds(0, 3), :, lower], ox_recv.at[l, 1])
         share = jnp.zeros((16, 256), F32)
         for group in TP_GROUPS:
             wait_bytes(gat_in.at[l, pl.ds(0, 4)], c_recv.at[l, group])
             heads = [gat_in[l, 4 * group + i] for i in range(4)]
             rows = jnp.concatenate(heads, axis=1)
-            columns = wout[l, 4 * group : 4 * group + 4].reshape(512, 256)
+            columns = wout[l, group].reshape(512, 256)
             share += jnp.dot(rows, columns, preferred_element_type=F32)
         before = cur[0] if l == 0 else held[...]
         fresh = (before.astype(F32) + share).astype(BF16)
@@ -348,7 +376,6 @@
                 remote(held, target, e_send_pair, e_recv.at[0], partner).start()
                 wait_bytes(held, e_send_pair)
 
-            gather_weights(1)
         else:
             final[h] = fresh
             for to, _ in peers:
@@ -364,7 +391,9 @@
     for l in range(2):
         wait_bytes(sq_in.at[l, pl.ds(0, 7)], s2_send.at[l])
         wait_bytes(sums_in.at[l, pl.ds(0, 7)], a2_send.at[l])
-        wait_bytes(wout.at[l, pl.ds(0, 15)], o_send.at[l])
+        for sem in (ox_send, oy_send):
+            wait_bytes(wout.at[l, 0, pl.ds(0, 3), upper], sem.at[l, 0])
+            wait_bytes(wout.at[l, pl.ds(0, 3), :, upper], sem.at[l, 1])
 
         @pl.when(h == d)
         def _():
@@ -411,7 +440,7 @@
             pltpu.VMEM((2, 256, 512), BF16),
             pltpu.VMEM((2, 128), F32),
             pltpu.VMEM((2, 128), F32),
-            pltpu.VMEM((2, 16, 128, 256), BF16),
+            pltpu.VMEM((2, 4, 4, 128, 256), BF16),
             pltpu.VMEM((2, 16, 128, 128), F32),
             pltpu.VMEM((16, 16, 512), BF16),
             pltpu.VMEM((8, 16, 512), BF16),
@@ -440,8 +469,10 @@
             dma((2,)),
             dma((2,)),
             dma((2, 4)),
-            dma((2,)),
-            dma((2,)),
+            dma((2, 2)),
+            dma((2, 2)),
+            dma((2, 2)),
+            dma((2, 2)),
             dma((2,)),
             dma((2,)),
             dma,

time: 60.8 us -> 51.3 us (0.84)
  Pallas kernels: 60 us -> 50.5 us
    pallas_call x1, Pallas kernels: 58.6 us -> 49.1 us  [per_device(): pl.pallas_call(kernel, out_shape=tuple((pltpu.VMEM(shape, dtype) for shap...]
where the time goes in v5:
time: 51.3 us; the launch traced here: 51.1 us
  Pallas kernels  50.5 us (98%)
  between operations  0.64 us (1%)
    pallas_call x1, Pallas kernels, per_device(): pl.pallas_call(kernel, out_shape=tuple((pltpu.VMEM(shape, dtype) for shap...  49.1 us
    pallas_call x1, Pallas kernels, per_device(): pl.pallas_call(write_out, out_shape=tuple((jax.ShapeDtypeStruct(shape, dt...  1.43 us

profile of v5, /device:TPU:1, one launch (start us, length us, event | category | flops | bytes accessed | tf_op | source)
XLA Modules:
  0.0 51.1 jit_solution(13435943697371009712)
XLA Ops:
  0.6 49.1 %shard_map.113 = (bf16[256,256]{1,0:T(8,128)(2,1)S(1)}, f32[2,16,1,128,128]{4,3,2,1,0:T(8,128)S(1)}) custom-call(bf16[256,256]{1,0:T(8,128)(2,1)} %tok_in.1, f32[2,256]{1,0:T(2,128)} %gain_in.1, bf16[2,256,128]{2,1,0:T(8,128)(2,1)} %wq_in.1, bf16[2,256,128]{2,1,0:T(8,128)(2,1)} %wf_in.1, bf16[2,256,128]{2,1,0:T(8,128)(2,1)} %wv_in.1, ...), custom_call_target="tpu_custom_call" | custom-call | tf_op jit(solution)/shard_map/pallas_call | solution.py:428
  49.7 1.4 %shard_map.114 = (bf16[256,256]{1,0:T(8,128)(2,1)}, f32[2,16,1,128,128]{4,3,2,1,0:T(8,128)}) custom-call(bf16[256,256]{1,0:T(8,128)(2,1)S(1)} %get-tuple-element.4.mixed, f32[2,16,1,128,128]{4,3,2,1,0:T(8,128)S(1)} %get-tuple-element.5.state), custom_call_target="tpu_custom_call" | custom-call | tf_op jit(solution)/shard_map/pallas_call | solution.py:483

commit v6 on v5

--- a/solution.py
+++ b/solution.py
@@ -16,6 +16,9 @@
 
 Z_FAR = (4, 3, 5, 2, 6, 1, 7, 0)
 TP_GROUPS = (0, 2, 3, 1)
+
+
+SERVED = ((1, 1), (1, 3), (0, 2), (0, 1), (0, 3), (1, 0), (3, 0))
 
 
 def gray(v):
@@ -113,34 +116,29 @@
     load("gain", gain_in, gain)
     for n in range(4):
         load(("w", 0, n), weights[n].at[0], w0.at[:, pl.ds(128 * n, 128)])
+    def tp_at(dy, dx):
+        return ((y + dy) % 4) * 4 + (x + dx) % 4
+
+    antipode = tp_at(2, 2)
+    owners = (d, ((d // 4 + 2) % 4) * 4 + (d % 4 + 2) % 4)
+    own_copies = jnp.where((owners[0] == h) | (owners[1] == h), 1, 0)
+
     barrier = pltpu.get_barrier_semaphore()
-    for k in range(1, 16):
-        to = (h + k) % 16
-        pl.semaphore_signal(barrier, inc=1, device_id={"dp": (d + k) % 16}, device_id_type=MESH)
-        pl.semaphore_signal(barrier, inc=1, device_id={"tp": to}, device_id_type=MESH)
-        across = {"tp": to, **partner}
-        pl.semaphore_signal(barrier, inc=1, device_id=across, device_id_type=MESH)
-        away = {"tp": to, "dp": h}
-        pl.semaphore_signal(barrier, inc=1, device_id=away, device_id_type=MESH)
-
-    @pl.when(h != d)
-    def _():
-        pl.semaphore_signal(barrier, inc=1, device_id={"dp": h}, device_id_type=MESH)
-
+
+    def greet(device):
+        pl.semaphore_signal(barrier, inc=1, device_id=device, device_id_type=MESH)
+
+    for n in range(1, 8):
+        greet({"dp": (d + 2 * n) % 16})
+    greet(partner)
+    for n in range(1, 16):
+        greet({"tp": (h + n) % 16})
 
     own = pl.multiple_of(8 * e, 8)
     other = pl.multiple_of(8 - 8 * e, 8)
     self_dy = ((2 * z + core) // 4 - y + 4) % 4
     self_dx = ((2 * z + core) % 4 - x + 4) % 4
     self_slot = (self_dx // 2) * 4 + gray(self_dy)
-    own_slot = tp_slot((y - d // 4 + 4) % 4, (x - d % 4 + 4) % 4)
-    near = (0, 1, 2, 1)
-    offsets = [(dy, dx) for dy in range(4) for dx in range(4) if dy or dx]
-    offsets.sort(key=lambda o: -near[o[0]] - near[o[1]])
-    peers = [
-        (((y + dy) % 4) * 4 + (x + dx) % 4, tp_slot((4 - dy) % 4, (4 - dx) % 4)) for dy, dx in offsets
-    ]
-
     def remote(src, dst, send, recv, device):
         return pltpu.make_async_remote_copy(
             src_ref=src,
@@ -238,7 +236,7 @@
             load(("wout", 1), wout_in.at[1], wout.at[1, 0, 0])
             for c in range(2):
                 sq[c] = squares(cur[8 * c : 8 * c + 8].astype(F32).reshape(128, 256))
-            pl.semaphore_wait(barrier, jnp.where(h == d, 60, 61))
+            pl.semaphore_wait(barrier, 23)
             remote(sq.at[1 - e], sq_pair_in, s1_send, s1_recv, partner).start()
             for half in range(2):
                 remote(
@@ -310,21 +308,29 @@
         gated = read * hgain[l : l + 1, :] * jax.nn.silu(gate_pre)
         gat[l] = gated.astype(BF16)
 
-        landing = gat_in.at[l, own_slot]
-        recv = c_recv.at[l, own_slot // 4]
+        places = []
+        for b, owner in enumerate(owners):
+            slot = tp_slot((y - owner // 4 + 4) % 4, (x - owner % 4 + 4) % 4)
+            places.append((owner, gat_in.at[l, 16 * b + slot], c_recv.at[l, slot // 4]))
+
+        def send_read(owner, landing, recv, to):
+            remote(gat.at[l], landing, c_send.at[l], recv, {"tp": owner, "dp": to}).start()
+
         for dz in Z_FAR:
             for other_core in (1, 0):
                 to = 2 * ((z + dz) % 8) + (core + other_core) % 2
-
-                @pl.when((h != d) | (to != d))
-                def _():
-                    remote(
-                        gat.at[l], landing, c_send.at[l], recv, {"tp": d, "dp": to}
-                    ).start()
-
-        @pl.when(h == d)
-        def _():
-            pltpu.make_async_copy(gat.at[l], landing, recv).start()
+                for owner, landing, recv in places:
+                    if dz or other_core:
+                        send_read(owner, landing, recv, to)
+                        continue
+
+                    @pl.when(owner != h)
+                    def _():
+                        send_read(owner, landing, recv, to)
+
+                    @pl.when(owner == h)
+                    def _():
+                        pltpu.make_async_copy(gat.at[l], landing, recv).start()
 
         if l == 0:
             for n in range(4):
@@ -343,45 +349,51 @@
 
         wait_bytes(wout.at[l, pl.ds(0, 3), :, upper], oy_recv.at[l, 1])
         wait_bytes(wout.at[l, pl.ds(0, 3), :, lower], ox_recv.at[l, 1])
-        share = jnp.zeros((16, 256), F32)
+        share = jnp.zeros((32, 256), F32)
         for group in TP_GROUPS:
-            wait_bytes(gat_in.at[l, pl.ds(0, 4)], c_recv.at[l, group])
-            heads = [gat_in[l, 4 * group + i] for i in range(4)]
-            rows = jnp.concatenate(heads, axis=1)
+            wait_bytes(gat_in.at[l, pl.ds(0, 8)], c_recv.at[l, group])
+            rows = [
+                jnp.concatenate([gat_in[l, 16 * b + 4 * group + i] for i in range(4)], axis=1)
+                for b in range(2)
+            ]
+            rows = jnp.concatenate(rows, axis=0)
             columns = wout[l, group].reshape(512, 256)
             share += jnp.dot(rows, columns, preferred_element_type=F32)
-        before = cur[0] if l == 0 else held[...]
-        fresh = (before.astype(F32) + share).astype(BF16)
+        before = [cur[0], cur[tp_slot(2, 2)]] if l == 0 else [held[0], held[1]]
+        before = jnp.concatenate(before, axis=0).astype(F32)
+        fresh = (before + share).astype(BF16).reshape(2, 16, 256)
 
         if l == 0:
             held[...] = fresh
-            to_core = x % 2
-            for to, tp_slot_there in peers:
-                slot = tp_slot_there % 8
-                remote(
-                    held,
-                    cur1.at[slot, :, pl.ds(256 * core, 256)],
-                    e_send.at[0],
-                    e_recv.at[slot // 4],
-                    {"tp": to, "dp": 2 * z + to_core},
-                ).start()
-            target = cur1.at[0, :, pl.ds(256 * core, 256)]
-
-            @pl.when(to_core == core)
-            def _():
-                pltpu.make_async_copy(held, target, e_recv.at[0]).start()
-
-            @pl.when(to_core != core)
-            def _():
-                remote(held, target, e_send_pair, e_recv.at[0], partner).start()
-                wait_bytes(held, e_send_pair)
+            for dy, dx in SERVED:
+                for b in range(2):
+                    slot = tp_slot((2 * b + 4 - dy) % 4, (2 * b + 4 - dx) % 4) % 8
+                    remote(
+                        held.at[b],
+                        cur1.at[slot, :, pl.ds(256 * core, 256)],
+                        e_send.at[0],
+                        e_recv.at[slot // 4],
+                        {"tp": tp_at(dy, dx), "dp": 2 * z + x % 2},
+                    ).start()
+            for b in range(2):
+                slot = tp_slot(2 * b, 2 * b) % 8
+                target = cur1.at[slot, :, pl.ds(256 * core, 256)]
+
+                @pl.when(x % 2 == core)
+                def _():
+                    pltpu.make_async_copy(held.at[b], target, e_recv.at[slot // 4]).start()
+
+                @pl.when(x % 2 != core)
+                def _():
+                    remote(held.at[b], target, e_send_pair, e_recv.at[slot // 4], partner).start()
 
         else:
-            final[h] = fresh
-            for to, _ in peers:
-                remote(
-                    final.at[h], final.at[h], e_send.at[1], final_recv, {"tp": to}
-                ).start()
+            final[h] = fresh[0]
+            final[antipode] = fresh[1]
+            for dy, dx in SERVED:
+                for block in (h, antipode):
+                    there = final.at[block]
+                    remote(there, there, e_send.at[1], final_recv, {"tp": tp_at(dy, dx)}).start()
 
     wait_bytes(sq_pair_in, s1_send)
     for half in range(2):
@@ -395,16 +407,21 @@
             wait_bytes(wout.at[l, 0, pl.ds(0, 3), upper], sem.at[l, 0])
             wait_bytes(wout.at[l, pl.ds(0, 3), :, upper], sem.at[l, 1])
 
-        @pl.when(h == d)
+        @pl.when(own_copies == 1)
         def _():
-            wait_bytes(gat_in.at[l, pl.ds(0, 15)], c_send.at[l])
-
-        @pl.when(h != d)
+            wait_bytes(gat_in.at[l, pl.ds(0, 31)], c_send.at[l])
+
+        @pl.when(own_copies == 0)
         def _():
             wait_bytes(gat_in.at[l], c_send.at[l])
 
-        wait_bytes(cur.at[pl.ds(0, 15)], e_send.at[l])
-    wait_bytes(final.at[pl.ds(0, 15)], final_recv)
+        wait_bytes(cur.at[pl.ds(0, 14)], e_send.at[l])
+
+    @pl.when(x % 2 != core)
+    def _():
+        wait_bytes(held, e_send_pair)
+
+    wait_bytes(final.at[pl.ds(0, 14)], final_recv)
     mixed_out[...] = final[...].reshape(256, 256)
 
 
@@ -433,7 +450,7 @@
         scratch_shapes=[
             pltpu.VMEM((16, 16, 256), BF16),
             pltpu.VMEM((8, 16, 512), BF16),
-            pltpu.VMEM((16, 256), BF16),
+            pltpu.VMEM((2, 16, 256), BF16),
             pltpu.VMEM((2, 256), F32),
             pltpu.VMEM((2, 1, 256), F32),
             pltpu.VMEM((256, 512), BF16),
@@ -451,7 +468,7 @@
             pltpu.VMEM((2, 1, 128), F32),
             pltpu.VMEM((2, 8, 1, 128), F32),
             pltpu.VMEM((2, 16, 128), BF16),
-            pltpu.VMEM((2, 16, 16, 128), BF16),
+            pltpu.VMEM((2, 32, 16, 128), BF16),
             pltpu.VMEM((16, 16, 256), BF16),
             dma((17,)),
             dma,

time: 51.3 us -> 49.9 us (0.973)
  Pallas kernels: 50.5 us -> 49.1 us
    pallas_call x1, Pallas kernels: 49.1 us -> 47.7 us  [per_device(): pl.pallas_call(kernel, out_shape=tuple((pltpu.VMEM(shape, dtype) for shap...]
where the time goes in v6:
time: 49.9 us; the launch traced here: 49.7 us
  Pallas kernels  49.1 us (98%)
  between operations  0.64 us (1%)
    pallas_call x1, Pallas kernels, per_device(): pl.pallas_call(kernel, out_shape=tuple((pltpu.VMEM(shape, dtype) for shap...  47.7 us
    pallas_call x1, Pallas kernels, per_device(): pl.pallas_call(write_out, out_shape=tuple((jax.ShapeDtypeStruct(shape, dt...  1.43 us

profile of v6, /device:TPU:1, one launch (start us, length us, event | category | flops | bytes accessed | tf_op | source)
XLA Modules:
  0.0 49.7 jit_solution(16513786356942015792)
XLA Ops:
  0.6 47.7 %shard_map.113 = (bf16[256,256]{1,0:T(8,128)(2,1)S(1)}, f32[2,16,1,128,128]{4,3,2,1,0:T(8,128)S(1)}) custom-call(bf16[256,256]{1,0:T(8,128)(2,1)} %tok_in.1, f32[2,256]{1,0:T(2,128)} %gain_in.1, bf16[2,256,128]{2,1,0:T(8,128)(2,1)} %wq_in.1, bf16[2,256,128]{2,1,0:T(8,128)(2,1)} %wf_in.1, bf16[2,256,128]{2,1,0:T(8,128)(2,1)} %wv_in.1, ...), custom_call_target="tpu_custom_call" | custom-call | tf_op jit(solution)/shard_map/pallas_call | solution.py:445
  48.3 1.4 %shard_map.114 = (bf16[256,256]{1,0:T(8,128)(2,1)}, f32[2,16,1,128,128]{4,3,2,1,0:T(8,128)}) custom-call(bf16[256,256]{1,0:T(8,128)(2,1)S(1)} %get-tuple-element.4.mixed, f32[2,16,1,128,128]{4,3,2,1,0:T(8,128)S(1)} %get-tuple-element.5.state), custom_call_target="tpu_custom_call" | custom-call | tf_op jit(solution)/shard_map/pallas_call | solution.py:500
